TPU v7x, 32 devices: a whole 2x2x4 slice. The times are simulated.
32 devices in a mesh: grp: 2 (over y), sp: 4 (over z), tp: 4 (over x, core).
Axes of the slice: x: 2, y: 2, z: 4, core: 2. Of those that a mesh axis runs over, the one named last changes fastest.
Arguments:
- residual: bfloat16 [2048, 2048], P(('grp', 'sp', 'tp')), parts along dimension 0, may hold values from -6 to 6
- queries_wide: bfloat16 [2048, 1024], P(('grp', 'sp'), 'tp'), parts along dimension 0, may hold values from -6 to 6
- keys_wide: bfloat16 [2048, 512], P(('grp', 'sp'), 'tp'), parts along dimension 0, may hold values from -6 to 6
- values_wide: bfloat16 [2048, 512], P(('grp', 'sp'), 'tp'), parts along dimension 0, may hold values from -6 to 6
- queries_narrow: bfloat16 [2048, 512], P(('grp', 'sp'), 'tp'), parts along dimension 0, may hold values from -6 to 6
- keys_narrow: bfloat16 [2048, 256], P(('grp', 'sp'), 'tp'), parts along dimension 0, may hold values from -6 to 6
- values_narrow: bfloat16 [2048, 256], P(('grp', 'sp'), 'tp'), parts along dimension 0, may hold values from -6 to 6
- query_gain_wide: float32 [128], replicated, may hold values from 1 to 6
- key_gain_wide: float32 [128], replicated, may hold values from 1 to 6
- query_gain_narrow: float32 [64], replicated, may hold values from 1 to 6
- key_gain_narrow: float32 [64], replicated, may hold values from 1 to 6
- output_wide: bfloat16 [1024, 2048], P('tp'), may hold values from -0.3125 to 0.3125
- output_narrow: bfloat16 [512, 2048], P('tp'), may hold values from -0.3125 to 0.3125
- norm_gain: float32 [2048], replicated, may hold values from 0.1 to 1.9
- gate_weight: bfloat16 [4, 2048, 3584], P('sp', None, 'tp'), may hold values from -0.125 to 0.125
- up_weight: bfloat16 [4, 2048, 3584], P('sp', None, 'tp'), may hold values from -0.125 to 0.125
- down_weight: bfloat16 [4, 3584, 2048], P('sp', 'tp'), may hold values from -0.09375 to 0.09375
- route_ids: int32 [2048, 2], P(('grp', 'sp', 'tp')), parts along dimension 0, may hold values from 0 to 3, all different within a row; in each aligned block of 64 rows (0 to 63, 64 to 127, ...) at most 64 rows name the same one
- route_weights: float32 [2048, 2], P(('grp', 'sp', 'tp')), parts along dimension 0, may hold values from 0.1 to 0.9
Outputs:
- result: bfloat16 [2048, 2048], P(('grp', 'sp', 'tp')), parts along dimension 0
There are 2 independent parts, one for each index of `grp`. A program takes and returns all parts, laid end to end along the dimension named above; an argument that names none is the same for every part. Nothing has to cross between parts.
Inputs may be any that keep to these rules, and one draw needn't show every extreme that they name: `route_ids`: in each aligned block of 64 rows (the rows of one device) no expert is named by more than 64 rows, a bound that some block reaches; a row names 2 different experts.
All inputs are finite; a program needn't handle non-finite values.
Results may differ from a plain program's by a relative error of at most 0.013.
The roundings to bfloat16 on the way count: a program that leaves them out, or rounds other values in their place, can miss the bound.
Values may be sent and summed in bfloat16 or wider, within the bound.
No kernel may reach another device: no remote copies, remote signals or barrier semaphores. Data moves between devices by JAX's collectives and lax.ppermute only.
A program may use at most 128 MiB of HBM per device.

v0:
```python
import functools

import jax
import jax.numpy as jnp
import numpy as np
from jax import lax
from jax.experimental import pallas as pl
from jax.experimental.pallas import tpu as pltpu
from jax.sharding import PartitionSpec as P

GRID = 64


THETA = 10000.0
EPS = 1e-06
NEG_BIG = -1e30


def rotary_tables(places, head_width):
    quarter = head_width // 4
    inv_freq = THETA ** (-jnp.arange(quarter, dtype=jnp.float32) / quarter)
    grid_rows = (places // GRID).astype(jnp.float32)
    grid_cols = (places % GRID).astype(jnp.float32)
    row_angle = grid_rows[:, None] * inv_freq[None, :]
    col_angle = grid_cols[:, None] * inv_freq[None, :]
    angles = jnp.concatenate([row_angle, row_angle, col_angle, col_angle], axis=-1)
    return (jnp.cos(angles), jnp.sin(angles))


def head_norm_rotate(values, gain_vec, cos_table, sin_table):
    as_float = values.astype(jnp.float32)
    scaled = as_float * lax.rsqrt(jnp.mean(as_float * as_float, axis=-1, keepdims=True) + EPS)
    scaled = scaled * gain_vec
    full_shape = scaled.shape
    quarter = full_shape[-1] // 4
    halves = scaled.reshape(full_shape[:-1] + (2, 2, quarter))
    turned = jnp.stack([-halves[..., 1, :], halves[..., 0, :]], axis=-2).reshape(full_shape)
    return (scaled * cos_table[:, None, :] + turned * sin_table[:, None, :]).astype(jnp.bfloat16)


def fresh_state(queries):
    key_heads, group_size, tok_count = (queries.shape[1], queries.shape[2], queries.shape[0])
    return (
        jnp.full((key_heads, group_size, tok_count), NEG_BIG, jnp.float32),
        jnp.zeros((key_heads, group_size, tok_count), jnp.float32),
        jnp.zeros(queries.shape, jnp.float32),
    )


def key_sweep(carried, queries, keys, values):
    key_count = keys.shape[0]
    key_heads = queries.shape[1]
    head_width = queries.shape[3]
    block_len = 2048 if key_count % 2048 == 0 else key_count
    key_blocks = keys.reshape(key_count // block_len, block_len, key_heads, head_width)
    value_blocks = values.reshape(key_count // block_len, block_len, key_heads, head_width)
    score_scale = head_width ** (-0.5)

    def step(carried_state, blocks_in):
        key_block, value_block = blocks_in
        running_max, weight_sum, weighted = carried_state
        scores = (
            jnp.einsum("qhgd,khd->hgqk", queries, key_block, preferred_element_type=jnp.float32)
            * score_scale
        )
        new_max = jnp.maximum(running_max, jnp.max(scores, axis=-1))
        weights = jnp.exp(scores - new_max[..., None])
        rescale = jnp.exp(running_max - new_max)
        weight_sum = weight_sum * rescale + jnp.sum(weights, axis=-1)
        mixed_values = jnp.einsum(
            "hgqk,khd->qhgd",
            weights.astype(jnp.bfloat16),
            value_block,
            preferred_element_type=jnp.float32,
        )
        weighted = weighted * jnp.transpose(rescale, (2, 0, 1))[..., None] + mixed_values
        return ((new_max, weight_sum, weighted), None)

    carried, _ = lax.scan(step, carried, (key_blocks, value_blocks))
    return carried


def finish_heads(carried):
    weighted = carried[2]
    outcome = weighted / jnp.transpose(carried[1], (2, 0, 1))[..., None]
    return outcome.astype(jnp.bfloat16).reshape(weighted.shape[0], -1)


def slot_tables(chosen, slot_count, expert_count):
    row_count = chosen.shape[0]
    pick_count = chosen.shape[1]
    flat_pick = chosen.reshape(row_count * pick_count)
    hit_marks = (flat_pick[:, None] == jnp.arange(expert_count, dtype=jnp.int32)[None, :]).astype(
        jnp.int32
    )
    before = jnp.cumsum(hit_marks, axis=0) - hit_marks
    slot_place = jnp.sum(before * hit_marks, axis=1)
    target = flat_pick * slot_count + slot_place
    slot_table = target[:, None] == jnp.arange(expert_count * slot_count, dtype=jnp.int32)[None, :]
    return slot_table.astype(jnp.bfloat16).reshape(row_count, pick_count, expert_count * slot_count)


def routed_body(
    residual,
    queries_wide,
    keys_wide,
    values_wide,
    queries_narrow,
    keys_narrow,
    values_narrow,
    query_gain_wide,
    key_gain_wide,
    query_gain_narrow,
    key_gain_narrow,
    output_wide,
    output_narrow,
    norm_gain,
    gate_weight,
    up_weight,
    down_weight,
    route_ids,
    route_weights,
):
    tok_count = queries_wide.shape[0]
    places = lax.axis_index("sp") * tok_count + jnp.arange(tok_count, dtype=jnp.int32)
    wide_width = query_gain_wide.shape[0]
    narrow_width = query_gain_narrow.shape[0]
    cos_wide, sin_wide = rotary_tables(places, wide_width)
    cos_narrow, sin_narrow = rotary_tables(places, narrow_width)
    wide_keyheads = keys_wide.shape[1] // wide_width
    narrow_keyheads = keys_narrow.shape[1] // narrow_width
    q_wide = head_norm_rotate(
        queries_wide.reshape(tok_count, -1, wide_width), query_gain_wide, cos_wide, sin_wide
    )
    q_wide = q_wide.reshape(tok_count, wide_keyheads, -1, wide_width)
    k_wide = head_norm_rotate(
        keys_wide.reshape(tok_count, -1, wide_width), key_gain_wide, cos_wide, sin_wide
    )
    k_wide = k_wide.reshape(tok_count, -1)
    q_narrow = head_norm_rotate(
        queries_narrow.reshape(tok_count, -1, narrow_width),
        query_gain_narrow,
        cos_narrow,
        sin_narrow,
    )
    q_narrow = q_narrow.reshape(tok_count, narrow_keyheads, -1, narrow_width)
    k_narrow = head_norm_rotate(
        keys_narrow.reshape(tok_count, -1, narrow_width), key_gain_narrow, cos_narrow, sin_narrow
    )
    k_narrow = k_narrow.reshape(tok_count, -1)
    carried = (fresh_state(q_wide), fresh_state(q_narrow))
    carried = (
        key_sweep(
            carried[0],
            q_wide,
            lax.all_gather(k_wide, "sp", axis=0, tiled=True),
            lax.all_gather(values_wide, "sp", axis=0, tiled=True),
        ),
        key_sweep(
            carried[1],
            q_narrow,
            lax.all_gather(k_narrow, "sp", axis=0, tiled=True),
            lax.all_gather(values_narrow, "sp", axis=0, tiled=True),
        ),
    )
    heads_wide = finish_heads(carried[0])
    heads_narrow = finish_heads(carried[1])
    own_rows = residual.shape[0]
    mixed_heads = lax.psum_scatter(
        (
            jnp.dot(heads_wide, output_wide, preferred_element_type=jnp.float32)
            + jnp.dot(heads_narrow, output_narrow, preferred_element_type=jnp.float32)
        ).astype(jnp.bfloat16),
        "tp",
        scatter_dimension=0,
        tiled=True,
    ).astype(jnp.float32)
    attended = (residual.astype(jnp.float32) + mixed_heads).astype(jnp.bfloat16)
    state_float = attended.astype(jnp.float32)
    normed = (
        state_float
        * lax.rsqrt(jnp.mean(state_float * state_float, axis=-1, keepdims=True) + EPS)
        * norm_gain
    ).astype(jnp.bfloat16)
    pick_count = route_ids.shape[1]
    expert_count = lax.axis_size("sp")
    slot_count = 2 * pick_count * own_rows // expert_count
    model_width = residual.shape[1]
    own_tables = slot_tables(route_ids, slot_count, expert_count)
    send_rows = jnp.einsum(
        "rks,rd->sd", own_tables, normed, preferred_element_type=jnp.float32
    ).astype(jnp.bfloat16)
    send_rows = send_rows.reshape(expert_count, slot_count, model_width)
    arrived = lax.all_to_all(send_rows, "sp", split_axis=0, concat_axis=0, tiled=True)
    copies = lax.all_gather(arrived, "tp", axis=0, tiled=True)
    expert_arrived = copies.reshape((lax.axis_size("tp"),) + arrived.shape)
    full_shape = expert_arrived.shape
    flat_rows = expert_arrived.reshape(-1, model_width)
    gate_act = jnp.dot(flat_rows, gate_weight[0], preferred_element_type=jnp.float32)
    up_act = jnp.dot(flat_rows, up_weight[0], preferred_element_type=jnp.float32)
    hidden = (jax.nn.silu(gate_act) * up_act).astype(jnp.bfloat16)
    partial_value = jnp.dot(hidden, down_weight[0], preferred_element_type=jnp.float32).reshape(
        full_shape
    )
    summed = lax.psum_scatter(
        partial_value.astype(jnp.bfloat16), "tp", scatter_dimension=0, tiled=True
    ).astype(jnp.float32)
    results = summed.reshape(full_shape[1:]).astype(jnp.bfloat16)
    returned = lax.all_to_all(results, "sp", split_axis=0, concat_axis=0, tiled=True)
    returned_flat = returned.reshape(expert_count * slot_count, model_width)
    picked = jnp.einsum(
        "rks,sd->rkd", own_tables, returned_flat, preferred_element_type=jnp.float32
    )
    mixture = jnp.sum(route_weights[:, :, None] * picked, axis=1)
    return (state_float + mixture).astype(jnp.bfloat16)


VMEM_SPEC = pl.BlockSpec(memory_space=pltpu.VMEM)
MIB = 2**20
WAIT_FLOPS = 8 * 10**9


def on_core(kernel, results, args, flops=0, exps=0, vmem=24):
    moved = sum(a.size * a.dtype.itemsize for a in list(args) + list(results))
    return pl.pallas_call(
        kernel,
        out_shape=results,
        in_specs=[VMEM_SPEC] * len(args),
        out_specs=[VMEM_SPEC] * len(results),
        compiler_params=pltpu.CompilerParams(vmem_limit_bytes=vmem * MIB),
        cost_estimate=pl.CostEstimate(
            flops=int(flops), bytes_accessed=int(moved), transcendentals=int(exps)
        ),
    )(*args)


def like(rows, cols, dtype=jnp.bfloat16):
    return jax.ShapeDtypeStruct((rows, cols), dtype)


def lanes_of(shape):
    return lax.broadcasted_iota(jnp.int32, shape, 1)


def turned(values, quarter):
    width = values.shape[1]
    ahead = pltpu.roll(values, width - quarter, 1)
    behind = pltpu.roll(values, quarter, 1)
    return jnp.where(lanes_of(values.shape) % (2 * quarter) < quarter, ahead, behind)


def rotated(scaled, quarter, cos_table, sin_table):
    return (scaled * cos_table + turned(scaled, quarter) * sin_table).astype(jnp.bfloat16)


def rms(values, width):
    return lax.rsqrt(jnp.sum(values * values, axis=1, keepdims=True) / width + EPS)


def packed(wide_pair, narrow_pair):
    return jnp.concatenate(
        [jnp.concatenate(wide_pair, axis=1)] + [a.T for a in narrow_pair], axis=0
    )


def prepare_kernel(
    order,
    own_rows,
    qw_ref,
    qn_ref,
    small_ref,
    qw_out,
    qn_out,
    cw_ref,
    sw_ref,
    cn_ref,
    sn_ref,
):
    tokens, lanes = cw_ref.shape
    grid_rows = tokens // GRID
    for freq, width, cos_ref, sin_ref in (
        (small_ref[4:5, :], lanes, cw_ref, sw_ref),
        (small_ref[5:6, :], lanes // 2, cn_ref, sn_ref),
    ):
        row_at = lax.broadcasted_iota(jnp.int32, (grid_rows, lanes), 0).astype(jnp.float32) * freq
        col_at = lax.broadcasted_iota(jnp.int32, (GRID, lanes), 0).astype(jnp.float32) * freq
        quarter = width // 4
        row_cos, row_sin = jnp.cos(row_at), jnp.sin(row_at)
        col_cos, col_sin = jnp.cos(col_at), jnp.sin(col_at)
        lane = lanes_of((GRID, lanes))
        minus = lane % (2 * quarter) < quarter
        by_row = lane % width < width // 2
        for i in range(grid_rows):
            here = pl.ds(i * GRID, GRID)
            cos_ref[here, :] = jnp.where(by_row, row_cos[i : i + 1, :], col_cos)
            sines = jnp.where(by_row, row_sin[i : i + 1, :], col_sin)
            sin_ref[here, :] = jnp.where(minus, -sines, sines)
    sp, tp = lax.axis_index("sp"), lax.axis_index("tp")
    count = len(order) * own_rows
    gain_wide, gain_narrow = small_ref[0:1, :], small_ref[1:2, :]
    for slot, r in enumerate(order):
        source = pl.ds(pl.multiple_of((tp ^ r) * own_rows, own_rows), own_rows)
        place = pl.ds(pl.multiple_of(sp * count + (tp ^ r) * own_rows, own_rows), own_rows)
        target = pl.ds(slot * own_rows, own_rows)
        for h in range(qw_ref.shape[1] // lanes):
            head = pl.ds(h * lanes, lanes)
            value = qw_ref[source, head].astype(jnp.float32)
            value = value * rms(value, lanes) * gain_wide
            qw_out[target, head] = rotated(value, lanes // 4, cw_ref[place, :], sw_ref[place, :])
        value = qn_ref[source, :].astype(jnp.float32)
        low = lanes_of(value.shape) < lanes // 2
        first = rms(jnp.where(low, value, 0.0), lanes // 2)
        second = rms(jnp.where(low, 0.0, value), lanes // 2)
        value = value * jnp.where(low, first, second) * gain_narrow
        qn_out[target, :] = rotated(value, lanes // 8, cn_ref[place, :], sn_ref[place, :])


def mixed_in(query, keys, values, scale, before=None):
    scores = lax.dot_general(
        query, keys, (((1,), (1,)), ((), ())), preferred_element_type=jnp.float32
    )
    top = jnp.max(scores, axis=1, keepdims=True)
    if before is not None:
        top = jnp.maximum(top, before[0])
    weights = jnp.exp((scores - top) * scale)
    total = jnp.sum(weights, axis=1, keepdims=True)
    mixed = jnp.dot(weights.astype(jnp.bfloat16), values, preferred_element_type=jnp.float32)
    if before is not None:
        fade = jnp.exp((before[0] - top) * scale)
        total = total + before[1] * fade
        mixed = mixed + before[2] * fade
    return top, total, mixed


def keys_and_values(raw_refs, steps, small_ref, tables):
    cw_ref, sw_ref, cn_ref, sn_ref = tables
    lanes = small_ref.shape[1]
    sp = lax.axis_index("sp")
    kw, vw, kn, vn = [], [], [], []
    for r, ref in zip(steps, raw_refs, strict=True):
        count = ref.shape[0] - lanes
        place = pl.ds(pl.multiple_of((sp ^ r) * count, count), count)
        value = ref[:count, :lanes].astype(jnp.float32)
        value = value * rms(value, lanes) * small_ref[2:3, :]
        kw.append(rotated(value, lanes // 4, cw_ref[place, :], sw_ref[place, :]))
        vw.append(ref[:count, lanes:])
        both = ref[count:, :].astype(jnp.float32).T
        low = lanes_of(both.shape) < lanes // 2
        other = pltpu.roll(both, lanes // 2, 1)
        value = jnp.where(low, both, other)
        value = value * rms(jnp.where(low, both, 0.0), lanes // 2) * small_ref[3:4, :]
        kn.append(rotated(value, lanes // 8, cn_ref[place, :], sn_ref[place, :]))
        vn.append(jnp.where(low, other, both).astype(jnp.bfloat16))
    return [jnp.concatenate(v, axis=0) for v in (kw, vw, kn, vn)]


def all_heads(qw_ref, qn_ref, keys, lanes, before=None):
    kw, vw, kn, vn = keys
    query = qn_ref[...]
    low = lanes_of(query.shape) < lanes // 2
    nothing = jnp.zeros_like(query)
    heads = [
        (qw_ref[:, h * lanes : (h + 1) * lanes], kw, vw, lanes**-0.5)
        for h in range(qw_ref.shape[1] // lanes)
    ]
    heads.append((jnp.where(low, query, nothing), kn, vn, (lanes // 2) ** -0.5))
    heads.append((jnp.where(low, nothing, query), kn, vn, (lanes // 2) ** -0.5))
    before = [None] * len(heads) if before is None else before
    return [mixed_in(*head, old) for head, old in zip(heads, before, strict=True)]


def attend_first_kernel(steps, *refs):
    raw_refs, refs = refs[: len(steps)], refs[len(steps) :]
    qw_ref, qn_ref, small_ref = refs[:3]
    stat_ref, mixed_ref = refs[7:]
    lanes = small_ref.shape[1]
    keys = keys_and_values(raw_refs, steps, small_ref, refs[3:7])
    states = all_heads(qw_ref, qn_ref, keys, lanes)
    lane = lanes_of(stat_ref.shape)
    stat = jnp.zeros(stat_ref.shape, jnp.float32)
    for h, (top, total, mixed) in enumerate(states):
        stat = jnp.where(lane == 2 * h, top, stat)
        stat = jnp.where(lane == 2 * h + 1, total, stat)
        mixed_ref[h] = mixed
    stat_ref[...] = stat


def attend_last_kernel(steps, *refs):
    raw_refs, refs = refs[: len(steps)], refs[len(steps) :]
    qw_ref, qn_ref, small_ref = refs[:3]
    stat_ref, mixed_ref, ow_ref, on_ref, keep_ref, send_ref = refs[7:]
    lanes = small_ref.shape[1]
    keys = keys_and_values(raw_refs, steps, small_ref, refs[3:7])
    before = [
        (stat_ref[:, 2 * h : 2 * h + 1], stat_ref[:, 2 * h + 1 : 2 * h + 2], mixed_ref[h])
        for h in range(mixed_ref.shape[0])
    ]
    states = all_heads(qw_ref, qn_ref, keys, lanes, before)
    heads = [mixed / total for _, total, mixed in states]
    low = lanes_of(heads[-1].shape) < lanes // 2
    narrow = jnp.where(low, heads[-2], heads[-1]).astype(jnp.bfloat16)
    wide = jnp.concatenate(heads[:-2], axis=1).astype(jnp.bfloat16)
    terms = jnp.dot(wide, ow_ref[...], preferred_element_type=jnp.float32)
    terms = terms + jnp.dot(narrow, on_ref[...], preferred_element_type=jnp.float32)
    terms = terms.astype(jnp.bfloat16)
    half = terms.shape[0] // 2
    keep_ref[...] = terms[:half]
    send_ref[...] = terms[half:]


def norm_kernel(res_ref, keep_ref, came_ref, crossed_ref, gain_ref, att_ref, normed_ref):
    rows = res_ref.shape[0]
    term = keep_ref[:rows, :].astype(jnp.float32) + came_ref[:rows, :].astype(jnp.float32)
    term = term + crossed_ref[...].astype(jnp.float32)
    attended = (res_ref[...].astype(jnp.float32) + term).astype(jnp.bfloat16)
    att_ref[...] = attended
    state = attended.astype(jnp.float32)
    normed_ref[...] = (state * rms(state, state.shape[1]) * gain_ref[...]).astype(jnp.bfloat16)


def expert_kernel(r0_ref, r2_ref, r1_ref, r3_ref, gate_ref, up_ref, down_ref, keep_ref, send_ref):
    rows = jnp.concatenate([ref[...] for ref in (r0_ref, r2_ref, r1_ref, r3_ref)], axis=0)
    gate_act = jnp.dot(rows, gate_ref[0], preferred_element_type=jnp.float32)
    up_act = jnp.dot(rows, up_ref[0], preferred_element_type=jnp.float32)
    hidden = (gate_act / (1.0 + jnp.exp(-gate_act)) * up_act).astype(jnp.bfloat16)
    piece = jnp.dot(hidden, down_ref[0], preferred_element_type=jnp.float32).astype(jnp.bfloat16)
    half = piece.shape[0] // 2
    keep_ref[...] = piece[:half]
    send_ref[...] = piece[half:]


def lane_freqs(width, lanes):
    quarter = width // 4
    freq = THETA ** (-np.arange(quarter, dtype=np.float64) / quarter)
    return jnp.asarray(np.tile(freq, lanes // quarter), jnp.float32)


def dense_body(
    residual,
    queries_wide,
    keys_wide,
    values_wide,
    queries_narrow,
    keys_narrow,
    values_narrow,
    query_gain_wide,
    key_gain_wide,
    query_gain_narrow,
    key_gain_narrow,
    output_wide,
    output_narrow,
    norm_gain,
    gate_weight,
    up_weight,
    down_weight,
    route_ids,
    route_weights,
):
    n_sp, n_tp = lax.axis_size("sp"), lax.axis_size("tp")
    sp = lax.axis_index("sp")
    tok_count, own_rows = queries_wide.shape[0], residual.shape[0]
    model_width = residual.shape[1]
    hidden_width = gate_weight.shape[2]
    lanes = query_gain_wide.shape[0]
    tokens = n_sp * tok_count
    order = [r for r in range(n_tp) if r % 2 == 0] + [r for r in range(n_tp) if r % 2]
    half = tok_count // 2

    def across(value, axis, step):
        size = lax.axis_size(axis)
        return lax.ppermute(value, axis, [(i, i ^ step) for i in range(size)])

    def spread(own):
        two = across(own, "sp", 2)
        one = across(own, "sp", 1)
        return [own, one, two, across(two, "sp", 1)]

    raw_blocks = spread(packed([keys_wide, values_wide], [keys_narrow, values_narrow]))

    table = like(tokens, lanes, jnp.float32)
    small = jnp.concatenate(
        [query_gain_wide, query_gain_narrow, query_gain_narrow]
        + [key_gain_wide, key_gain_narrow, key_gain_narrow]
        + [lane_freqs(lanes, lanes), lane_freqs(lanes // 2, lanes)]
    ).reshape(6, lanes)
    q_wide, q_narrow, *tables = on_core(
        functools.partial(prepare_kernel, order, own_rows),
        [like(*queries_wide.shape), like(*queries_narrow.shape)] + [table] * 4,
        [queries_wide, queries_narrow, small],
        flops=WAIT_FLOPS,
    )
    heads = queries_wide.shape[1] // lanes + queries_narrow.shape[1] // (lanes // 2)
    shared = [q_wide, q_narrow, small] + tables
    one_block = dict(flops=WAIT_FLOPS, exps=heads * tok_count**2)
    stat, mixed = on_core(
        functools.partial(attend_first_kernel, (0, 1, 2)),
        [
            like(tok_count, lanes, jnp.float32),
            jax.ShapeDtypeStruct((heads, tok_count, lanes), jnp.float32),
        ],
        raw_blocks[:3] + shared,
        **one_block,
    )
    keep, send = on_core(
        functools.partial(attend_last_kernel, (3,)),
        [like(half, model_width)] * 2,
        raw_blocks[3:] + shared + [stat, mixed, output_wide, output_narrow],
        **one_block,
    )
    came = across(send, "tp", 1)

    def crossing(keep, came):
        pair = keep[own_rows:].astype(jnp.float32) + came[own_rows:].astype(jnp.float32)
        return across(pair.astype(jnp.bfloat16), "tp", 2)

    attended, normed = on_core(
        norm_kernel,
        [like(own_rows, model_width)] * 2,
        [residual, keep, came, crossing(keep, came), norm_gain[None, :]],
    )

    total = attended.astype(jnp.float32)
    arrived = spread(normed)
    crossed_rows = []
    for r in range(n_sp):
        if r % 2:
            crossed_rows.append(across(crossed_rows[r - 1], "sp", 1))
        else:
            crossed_rows.append(across(arrived[r], "tp", 2))
        rows = [arrived[r], crossed_rows[r]]
        rows = rows + [across(rows[0], "tp", 1), across(rows[1], "tp", 1)]
        keep, send = on_core(
            expert_kernel,
            [like(half, model_width)] * 2,
            rows + [gate_weight, up_weight, down_weight],
            flops=6 * tok_count * model_width * hidden_width,
            exps=tok_count * hidden_width,
        )
        came = across(send, "tp", 1)
        crossed = crossing(keep, came).astype(jnp.float32)
        expert_out = keep[:own_rows].astype(jnp.float32) + came[:own_rows].astype(jnp.float32)
        expert_out = (expert_out + crossed).astype(jnp.bfloat16)
        if r:
            expert_out = across(expert_out, "sp", r)
        weight = jnp.sum(jnp.where(route_ids == (sp ^ r), route_weights, 0.0), axis=1)
        total = total + weight[:, None] * expert_out.astype(jnp.float32)
    return total.astype(jnp.bfloat16)


def body(*arrays):
    own_rows, pick_count = arrays[17].shape
    slot_count = 2 * pick_count * own_rows // lax.axis_size("sp")
    every_row_fits = slot_count >= own_rows and lax.axis_size("sp") == lax.axis_size("tp") == 4
    wide, narrow = arrays[7].shape[0], arrays[9].shape[0]
    one_key_head = arrays[2].shape[1] == wide and arrays[5].shape[1] == narrow
    full_lanes = wide == 128 and 2 * narrow == wide and arrays[4].shape[1] == wide
    whole_rows = arrays[1].shape[0] % GRID == 0 and own_rows % 8 == 0
    if every_row_fits and one_key_head and full_lanes and whole_rows:
        return dense_body(*arrays)
    return routed_body(*arrays)


def solution(mesh):
    return jax.shard_map(
        body,
        mesh=mesh,
        in_specs=(
            P(("grp", "sp", "tp"), None),
            P(("grp", "sp"), "tp"),
            P(("grp", "sp"), "tp"),
            P(("grp", "sp"), "tp"),
            P(("grp", "sp"), "tp"),
            P(("grp", "sp"), "tp"),
            P(("grp", "sp"), "tp"),
            P(),
            P(),
            P(),
            P(),
            P("tp", None),
            P("tp", None),
            P(),
            P("sp", None, "tp"),
            P("sp", None, "tp"),
            P("sp", "tp", None),
            P(("grp", "sp", "tp"), None),
            P(("grp", "sp", "tp"), None),
        ),
        out_specs=P(("grp", "sp", "tp"), None),
        check_vma=False,
    )
```

profile of v0, /device:TPU:8, one launch (start us, length us, event | category | flops | bytes accessed | tf_op | source)
XLA Modules:
  0.0 123.1 jit_solution(10902323102638699792)
XLA Ops:
  0.9 2.7 %collective-permute-start = (bf16[384,256]{1,0:T(8,128)(2,1)S(1)}, bf16[384,256]{1,0:T(8,128)(2,1)S(1)}, u32[]{:S(2)}, u32[]{:S(2)}) collective-permute-start(bf16[384,256]{1,0:T(8,128)(2,1)S(1)} %pad_maximum_fusion.refs_0_), channel_id=1, source_target_pairs={{0,8},{4,12},{8,0},{12,4},{1,9},{5,13},{9,1},{13,5},{2,10},{6,14},... | collective-permute-start | bytes 589832 | tf_op jit(solution)/shard_map/ppermute | solution.py:471
  8.1 3.8 %collective-permute-done.refs_2_ = bf16[384,256]{1,0:T(8,128)(2,1)S(1)} collective-permute-done((bf16[384,256]{1,0:T(8,128)(2,1)S(1)}, bf16[384,256]{1,0:T(8,128)(2,1)S(1)}, u32[]{:S(2)}, u32[]{:S(2)}) %collective-permute-start) | collective-permute-done | bytes 196640 | tf_op jit(solution)/shard_map/ppermute | solution.py:471
  13.3 3.1 %shard_map.200 = (f32[256,128]{1,0:T(8,128)S(1)}, f32[4,256,128]{2,1,0:T(8,128)S(1)}) custom-call(bf16[384,256]{1,0:T(8,128)(2,1)S(1)} %pad_maximum_fusion.refs_0_, bf16[384,256]{1,0:T(8,128)(2,1)S(1)} %collective-permute-done.2.refs_1_, bf16[384,256]{1,0:T(8,128)(2,1)S(1)} %collective-permute-done.refs_2_, ...), custom_call_target="tpu_custom_call" | custom-call | flops 8000000000 | bytes 3542016 | tf_op jit(solution)/shard_map/pallas_call | solution.py:225
  16.4 2.3 %collective-permute-done.1.refs_0_ = bf16[384,256]{1,0:T(8,128)(2,1)S(1)} collective-permute-done((bf16[384,256]{1,0:T(8,128)(2,1)S(1)}, bf16[384,256]{1,0:T(8,128)(2,1)S(1)}, u32[]{:S(2)}, u32[]{:S(2)}) %collective-permute-start.1) | collective-permute-done | bytes 196640 | tf_op jit(solution)/shard_map/ppermute | solution.py:471
  18.7 3.2 %shard_map.201 = (bf16[128,2048]{1,0:T(8,128)(2,1)S(1)}, bf16[128,2048]{1,0:T(8,128)(2,1)S(1)}) custom-call(bf16[384,256]{1,0:T(8,128)(2,1)S(1)} %collective-permute-done.1.refs_0_, bf16[256,256]{1,0:T(8,128)(2,1)S(1)} %get-tuple-element.25.refs_3_.refs_1_, bf16[256,128]{1,0:T(8,128)(2,1)S(1)} %get-tuple-element.26.refs_4_.refs_2_, f32[6,128]{1,0:T(8,128)S(1)} %bitcast.7, ...), custom_call_target="tpu_custom_call" | custom-call | flops 8000000000 | bytes 5770240 | tf_op jit(solution)/shard_map/pallas_call | solution.py:225
  22.0 1.9 %collective-permute-done.3.came_ref = bf16[128,2048]{1,0:T(8,128)(2,1)S(1)} collective-permute-done((bf16[128,2048]{1,0:T(8,128)(2,1)S(1)}, bf16[128,2048]{1,0:T(8,128)(2,1)S(1)}, u32[]{:S(2)}, u32[]{:S(2)}) %collective-permute-start.3) | collective-permute-done | bytes 524320 | tf_op jit(solution)/shard_map/ppermute | solution.py:471
  25.5 6.9 %collective-permute-done.4.crossed_ref = bf16[64,2048]{1,0:T(8,128)(2,1)S(1)} collective-permute-done((bf16[64,2048]{1,0:T(8,128)(2,1)S(1)}, bf16[64,2048]{1,0:T(8,128)(2,1)S(1)}, u32[]{:S(2)}, u32[]{:S(2)}) %collective-permute-start.4) | collective-permute-done | bytes 262176 | tf_op jit(solution)/shard_map/ppermute | solution.py:471
  34.2 3.4 %collective-permute-start.17 = (bf16[64,2048]{1,0:T(8,128)(2,1)S(1)}, bf16[64,2048]{1,0:T(8,128)(2,1)S(1)}, u32[]{:S(2)}, u32[]{:S(2)}) collective-permute-start(bf16[64,2048]{1,0:T(8,128)(2,1)S(1)} %get-tuple-element.36.r0_ref), channel_id=1, source_target_pairs={{0,8},{4,12},{8,0},{12,4},{1,9},{5,13},{9,1},{13,5},{2,10},{6,14},... | collective-permute-start | bytes 786440 | tf_op jit(solution)/shard_map/ppermute | solution.py:471
  37.9 2.3 %collective-permute-done.5.r2_ref = bf16[64,2048]{1,0:T(8,128)(2,1)S(1)} collective-permute-done((bf16[64,2048]{1,0:T(8,128)(2,1)S(1)}, bf16[64,2048]{1,0:T(8,128)(2,1)S(1)}, u32[]{:S(2)}, u32[]{:S(2)}) %collective-permute-start.5) | collective-permute-done | bytes 262176 | tf_op jit(solution)/shard_map/ppermute | solution.py:471
  40.8 6.9 %collective-permute-done.17.r0_ref = bf16[64,2048]{1,0:T(8,128)(2,1)S(1)} collective-permute-done((bf16[64,2048]{1,0:T(8,128)(2,1)S(1)}, bf16[64,2048]{1,0:T(8,128)(2,1)S(1)}, u32[]{:S(2)}, u32[]{:S(2)}) %collective-permute-start.17) | collective-permute-done | bytes 262176 | tf_op jit(solution)/shard_map/ppermute | solution.py:471
  48.3 2.4 %collective-permute-done.10.r0_ref = bf16[64,2048]{1,0:T(8,128)(2,1)S(1)} collective-permute-done((bf16[64,2048]{1,0:T(8,128)(2,1)S(1)}, bf16[64,2048]{1,0:T(8,128)(2,1)S(1)}, u32[]{:S(2)}, u32[]{:S(2)}) %collective-permute-start.10) | collective-permute-done | bytes 262176 | tf_op jit(solution)/shard_map/ppermute | solution.py:471
  51.4 4.9 %collective-permute-done.11.r2_ref = bf16[64,2048]{1,0:T(8,128)(2,1)S(1)} collective-permute-done((bf16[64,2048]{1,0:T(8,128)(2,1)S(1)}, bf16[64,2048]{1,0:T(8,128)(2,1)S(1)}, u32[]{:S(2)}, u32[]{:S(2)}) %collective-permute-start.11) | collective-permute-done | bytes 262176 | tf_op jit(solution)/shard_map/ppermute | solution.py:471
  56.3 3.4 %shard_map.203 = (bf16[128,2048]{1,0:T(8,128)(2,1)S(1)}, bf16[128,2048]{1,0:T(8,128)(2,1)S(1)}) custom-call(bf16[64,2048]{1,0:T(8,128)(2,1)S(1)} %get-tuple-element.36.r0_ref, bf16[64,2048]{1,0:T(8,128)(2,1)S(1)} %collective-permute-done.5.r2_ref, bf16[64,2048]{1,0:T(8,128)(2,1)S(1)} %collective-permute-done.6.r1_ref, ...), custom_call_target="tpu_custom_call" | custom-call | flops 2818572288 | bytes 13107200 | tf_op jit(solution)/shard_map/pallas_call | solution.py:225
  60.4 1.8 %collective-permute-start.25 = (bf16[64,2048]{1,0:T(8,128)(2,1)S(1)}, bf16[64,2048]{1,0:T(8,128)(2,1)S(1)}, u32[]{:S(2)}, u32[]{:S(2)}) collective-permute-start(bf16[64,2048]{1,0:T(8,128)(2,1)S(1)} %collective-permute-done.18.r2_ref), channel_id=1, source_target_pairs={{0,4},{4,0},{8,12},{12,8},{1,5},{5,1},{9,13},{13,9},{2,6},{6,2},{1... | collective-permute-start | bytes 786440 | tf_op jit(solution)/shard_map/ppermute | solution.py:471
  62.2 3.6 %shard_map.204 = (bf16[128,2048]{1,0:T(8,128)(2,1)S(1)}, bf16[128,2048]{1,0:T(8,128)(2,1)S(1)}) custom-call(bf16[64,2048]{1,0:T(8,128)(2,1)S(1)} %collective-permute-done.10.r0_ref, bf16[64,2048]{1,0:T(8,128)(2,1)S(1)} %collective-permute-done.11.r2_ref, bf16[64,2048]{1,0:T(8,128)(2,1)S(1)} %collective-permute-done.12.r1_ref, ...), custom_call_target="tpu_custom_call" | custom-call | flops 2818572288 | bytes 13107200 | tf_op jit(solution)/shard_map/pallas_call | solution.py:225
  66.4 2.6 %collective-permute-done.25.r2_ref = bf16[64,2048]{1,0:T(8,128)(2,1)S(1)} collective-permute-done((bf16[64,2048]{1,0:T(8,128)(2,1)S(1)}, bf16[64,2048]{1,0:T(8,128)(2,1)S(1)}, u32[]{:S(2)}, u32[]{:S(2)}) %collective-permute-start.25) | collective-permute-done | bytes 262176 | tf_op jit(solution)/shard_map/ppermute | solution.py:471
  69.1 3.4 %shard_map.205 = (bf16[128,2048]{1,0:T(8,128)(2,1)S(1)}, bf16[128,2048]{1,0:T(8,128)(2,1)S(1)}) custom-call(bf16[64,2048]{1,0:T(8,128)(2,1)S(1)} %collective-permute-done.17.r0_ref, bf16[64,2048]{1,0:T(8,128)(2,1)S(1)} %collective-permute-done.18.r2_ref, bf16[64,2048]{1,0:T(8,128)(2,1)S(1)} %collective-permute-done.19.r1_ref, ...), custom_call_target="tpu_custom_call" | custom-call | flops 2818572288 | bytes 13107200 | tf_op jit(solution)/shard_map/pallas_call | solution.py:225
  73.1 3.4 %shard_map.206 = (bf16[128,2048]{1,0:T(8,128)(2,1)S(1)}, bf16[128,2048]{1,0:T(8,128)(2,1)S(1)}) custom-call(bf16[64,2048]{1,0:T(8,128)(2,1)S(1)} %collective-permute-done.24.r0_ref, bf16[64,2048]{1,0:T(8,128)(2,1)S(1)} %collective-permute-done.25.r2_ref, bf16[64,2048]{1,0:T(8,128)(2,1)S(1)} %collective-permute-done.26.r1_ref, ...), custom_call_target="tpu_custom_call" | custom-call | flops 2818572288 | bytes 13107200 | tf_op jit(solution)/shard_map/pallas_call | solution.py:225
  79.6 12.0 %collective-permute-done.15 = bf16[64,2048]{1,0:T(8,128)(2,1)S(1)} collective-permute-done((bf16[64,2048]{1,0:T(8,128)(2,1)S(1)}, bf16[64,2048]{1,0:T(8,128)(2,1)S(1)}, u32[]{:S(2)}, u32[]{:S(2)}) %collective-permute-start.15) | collective-permute-done | bytes 262176 | tf_op jit(solution)/shard_map/ppermute | solution.py:471
  93.4 3.8 %collective-permute-done.22 = bf16[64,2048]{1,0:T(8,128)(2,1)S(1)} collective-permute-done((bf16[64,2048]{1,0:T(8,128)(2,1)S(1)}, bf16[64,2048]{1,0:T(8,128)(2,1)S(1)}, u32[]{:S(2)}, u32[]{:S(2)}) %collective-permute-start.22) | collective-permute-done | bytes 262176 | tf_op jit(solution)/shard_map/ppermute | solution.py:471
  97.3 2.0 %collective-permute-start.23 = (bf16[64,2048]{1,0:T(8,128)(2,1)S(1)}, bf16[64,2048]{1,0:T(8,128)(2,1)S(1)}, u32[]{:S(2)}, u32[]{:S(2)}) collective-permute-start(bf16[64,2048]{1,0:T(8,128)(2,1)S(1)} %add_convert_fusion.3), channel_id=1, source_target_pairs={{0,8},{4,12},{8,0},{12,4},{1,9},{5,13},{9,1},{13,5},{2,10},{6,14},... | collective-permute-start | bytes 786440 | tf_op jit(solution)/shard_map/ppermute | solution.py:471
  99.3 3.0 %collective-permute-done.29 = bf16[64,2048]{1,0:T(8,128)(2,1)S(1)} collective-permute-done((bf16[64,2048]{1,0:T(8,128)(2,1)S(1)}, bf16[64,2048]{1,0:T(8,128)(2,1)S(1)}, u32[]{:S(2)}, u32[]{:S(2)}) %collective-permute-start.29) | collective-permute-done | bytes 262176 | tf_op jit(solution)/shard_map/ppermute | solution.py:471
  103.3 11.9 %collective-permute-done.23 = bf16[64,2048]{1,0:T(8,128)(2,1)S(1)} collective-permute-done((bf16[64,2048]{1,0:T(8,128)(2,1)S(1)}, bf16[64,2048]{1,0:T(8,128)(2,1)S(1)}, u32[]{:S(2)}, u32[]{:S(2)}) %collective-permute-start.23) | collective-permute-done | bytes 262176 | tf_op jit(solution)/shard_map/ppermute | solution.py:471
  115.2 6.7 %collective-permute-done.30 = bf16[64,2048]{1,0:T(8,128)(2,1)S(1)} collective-permute-done((bf16[64,2048]{1,0:T(8,128)(2,1)S(1)}, bf16[64,2048]{1,0:T(8,128)(2,1)S(1)}, u32[]{:S(2)}, u32[]{:S(2)}) %collective-permute-start.30) | collective-permute-done | bytes 262176 | tf_op jit(solution)/shard_map/ppermute | solution.py:471
  (80 shorter events, 21.4 us)
Async XLA Ops:
  0.9 10.9 %collective-permute-start = (bf16[384,256]{1,0:T(8,128)(2,1)S(1)}, bf16[384,256]{1,0:T(8,128)(2,1)S(1)}, u32[]{:S(2)}, u32[]{:S(2)}) collective-permute-start(bf16[384,256]{1,0:T(8,128)(2,1)S(1)} %pad_maximum_fusion.refs_0_), channel_id=1, source_target_pairs={{0,8},{4,12},{8,0},{12,4},{1,9},{5,13},{9,1},{13,5},{2,10},{6,14},... | collective-permute-start | bytes 589832 | tf_op jit(solution)/shard_map/ppermute | solution.py:471
  3.6 9.7 %collective-permute-start.2 = (bf16[384,256]{1,0:T(8,128)(2,1)S(1)}, bf16[384,256]{1,0:T(8,128)(2,1)S(1)}, u32[]{:S(2)}, u32[]{:S(2)}) collective-permute-start(bf16[384,256]{1,0:T(8,128)(2,1)S(1)} %pad_maximum_fusion.refs_0_), channel_id=1, source_target_pairs={{0,4},{4,0},{8,12},{12,8},{1,5},{5,1},{9,13},{13,9},{2,6},{6,2},{1... | collective-permute-start | bytes 589832 | tf_op jit(solution)/shard_map/ppermute | solution.py:471
  24.0 8.4 %collective-permute-start.4 = (bf16[64,2048]{1,0:T(8,128)(2,1)S(1)}, bf16[64,2048]{1,0:T(8,128)(2,1)S(1)}, u32[]{:S(2)}, u32[]{:S(2)}) collective-permute-start(bf16[64,2048]{1,0:T(8,128)(2,1)S(1)} %add_convert_fusion.9), channel_id=1, source_target_pairs={{0,2},{1,3},{2,0},{3,1},{4,6},{5,7},{6,4},{7,5},{8,10},{9,11},{10,... | collective-permute-start | bytes 786440 | tf_op jit(solution)/shard_map/ppermute | solution.py:471
  34.2 13.5 %collective-permute-start.17 = (bf16[64,2048]{1,0:T(8,128)(2,1)S(1)}, bf16[64,2048]{1,0:T(8,128)(2,1)S(1)}, u32[]{:S(2)}, u32[]{:S(2)}) collective-permute-start(bf16[64,2048]{1,0:T(8,128)(2,1)S(1)} %get-tuple-element.36.r0_ref), channel_id=1, source_target_pairs={{0,8},{4,12},{8,0},{12,4},{1,9},{5,13},{9,1},{13,5},{2,10},{6,14},... | collective-permute-start | bytes 786440 | tf_op jit(solution)/shard_map/ppermute | solution.py:471
  37.6 10.7 %collective-permute-start.6 = (bf16[64,2048]{1,0:T(8,128)(2,1)S(1)}, bf16[64,2048]{1,0:T(8,128)(2,1)S(1)}, u32[]{:S(2)}, u32[]{:S(2)}) collective-permute-start(bf16[64,2048]{1,0:T(8,128)(2,1)S(1)} %get-tuple-element.36.r0_ref), channel_id=1, source_target_pairs={{0,1},{1,0},{2,3},{3,2},{4,5},{5,4},{6,7},{7,6},{8,9},{9,8},{10,11... | collective-permute-start | bytes 786440 | tf_op jit(solution)/shard_map/ppermute | solution.py:471
  37.6 13.1 %collective-permute-start.10 = (bf16[64,2048]{1,0:T(8,128)(2,1)S(1)}, bf16[64,2048]{1,0:T(8,128)(2,1)S(1)}, u32[]{:S(2)}, u32[]{:S(2)}) collective-permute-start(bf16[64,2048]{1,0:T(8,128)(2,1)S(1)} %get-tuple-element.36.r0_ref), channel_id=1, source_target_pairs={{0,4},{4,0},{8,12},{12,8},{1,5},{5,1},{9,13},{13,9},{2,6},{6,2},{1... | collective-permute-start | bytes 786440 | tf_op jit(solution)/shard_map/ppermute | solution.py:471
  40.2 11.2 %collective-permute-start.7 = (bf16[64,2048]{1,0:T(8,128)(2,1)S(1)}, bf16[64,2048]{1,0:T(8,128)(2,1)S(1)}, u32[]{:S(2)}, u32[]{:S(2)}) collective-permute-start(bf16[64,2048]{1,0:T(8,128)(2,1)S(1)} %collective-permute-done.5.r2_ref), channel_id=1, source_target_pairs={{0,1},{1,0},{2,3},{3,2},{4,5},{5,4},{6,7},{7,6},{8,9},{9,8},{10,11... | collective-permute-start | bytes 786440 | tf_op jit(solution)/shard_map/ppermute | solution.py:471
  40.2 16.1 %collective-permute-start.11 = (bf16[64,2048]{1,0:T(8,128)(2,1)S(1)}, bf16[64,2048]{1,0:T(8,128)(2,1)S(1)}, u32[]{:S(2)}, u32[]{:S(2)}) collective-permute-start(bf16[64,2048]{1,0:T(8,128)(2,1)S(1)} %collective-permute-done.5.r2_ref), channel_id=1, source_target_pairs={{0,4},{4,0},{8,12},{12,8},{1,5},{5,1},{9,13},{13,9},{2,6},{6,2},{1... | collective-permute-start | bytes 786440 | tf_op jit(solution)/shard_map/ppermute | solution.py:471
  47.7 12.6 %collective-permute-start.18 = (bf16[64,2048]{1,0:T(8,128)(2,1)S(1)}, bf16[64,2048]{1,0:T(8,128)(2,1)S(1)}, u32[]{:S(2)}, u32[]{:S(2)}) collective-permute-start(bf16[64,2048]{1,0:T(8,128)(2,1)S(1)} %collective-permute-done.17.r0_ref), channel_id=1, source_target_pairs={{0,2},{1,3},{2,0},{3,1},{4,6},{5,7},{6,4},{7,5},{8,10},{9,11},{10,... | collective-permute-start | bytes 786440 | tf_op jit(solution)/shard_map/ppermute | solution.py:471
  48.3 17.6 %collective-permute-start.19 = (bf16[64,2048]{1,0:T(8,128)(2,1)S(1)}, bf16[64,2048]{1,0:T(8,128)(2,1)S(1)}, u32[]{:S(2)}, u32[]{:S(2)}) collective-permute-start(bf16[64,2048]{1,0:T(8,128)(2,1)S(1)} %collective-permute-done.17.r0_ref), channel_id=1, source_target_pairs={{0,1},{1,0},{2,3},{3,2},{4,5},{5,4},{6,7},{7,6},{8,9},{9,8},{10,11... | collective-permute-start | bytes 786440 | tf_op jit(solution)/shard_map/ppermute | solution.py:471
  50.7 9.7 %collective-permute-start.24 = (bf16[64,2048]{1,0:T(8,128)(2,1)S(1)}, bf16[64,2048]{1,0:T(8,128)(2,1)S(1)}, u32[]{:S(2)}, u32[]{:S(2)}) collective-permute-start(bf16[64,2048]{1,0:T(8,128)(2,1)S(1)} %collective-permute-done.17.r0_ref), channel_id=1, source_target_pairs={{0,4},{4,0},{8,12},{12,8},{1,5},{5,1},{9,13},{13,9},{2,6},{6,2},{1... | collective-permute-start | bytes 786440 | tf_op jit(solution)/shard_map/ppermute | solution.py:471
  59.8 16.9 %collective-permute-start.8 = (bf16[128,2048]{1,0:T(8,128)(2,1)S(1)}, bf16[128,2048]{1,0:T(8,128)(2,1)S(1)}, u32[]{:S(2)}, u32[]{:S(2)}) collective-permute-start(bf16[128,2048]{1,0:T(8,128)(2,1)S(1)} %get-tuple-element.38), channel_id=1, source_target_pairs={{0,1},{1,0},{2,3},{3,2},{4,5},{5,4},{6,7},{7,6},{8,9},{9,8},{10,11... | collective-permute-start | bytes 1572872 | tf_op jit(solution)/shard_map/ppermute | solution.py:471
  60.3 8.7 %collective-permute-start.20 = (bf16[64,2048]{1,0:T(8,128)(2,1)S(1)}, bf16[64,2048]{1,0:T(8,128)(2,1)S(1)}, u32[]{:S(2)}, u32[]{:S(2)}) collective-permute-start(bf16[64,2048]{1,0:T(8,128)(2,1)S(1)} %collective-permute-done.18.r2_ref), channel_id=1, source_target_pairs={{0,1},{1,0},{2,3},{3,2},{4,5},{5,4},{6,7},{7,6},{8,9},{9,8},{10,11... | collective-permute-start | bytes 786440 | tf_op jit(solution)/shard_map/ppermute | solution.py:471
  60.4 8.6 %collective-permute-start.25 = (bf16[64,2048]{1,0:T(8,128)(2,1)S(1)}, bf16[64,2048]{1,0:T(8,128)(2,1)S(1)}, u32[]{:S(2)}, u32[]{:S(2)}) collective-permute-start(bf16[64,2048]{1,0:T(8,128)(2,1)S(1)} %collective-permute-done.18.r2_ref), channel_id=1, source_target_pairs={{0,4},{4,0},{8,12},{12,8},{1,5},{5,1},{9,13},{13,9},{2,6},{6,2},{1... | collective-permute-start | bytes 786440 | tf_op jit(solution)/shard_map/ppermute | solution.py:471
  62.2 10.9 %collective-permute-start.26 = (bf16[64,2048]{1,0:T(8,128)(2,1)S(1)}, bf16[64,2048]{1,0:T(8,128)(2,1)S(1)}, u32[]{:S(2)}, u32[]{:S(2)}) collective-permute-start(bf16[64,2048]{1,0:T(8,128)(2,1)S(1)} %collective-permute-done.24.r0_ref), channel_id=1, source_target_pairs={{0,1},{1,0},{2,3},{3,2},{4,5},{5,4},{6,7},{7,6},{8,9},{9,8},{10,11... | collective-permute-start | bytes 786440 | tf_op jit(solution)/shard_map/ppermute | solution.py:471
  65.9 11.5 %collective-permute-start.14 = (bf16[128,2048]{1,0:T(8,128)(2,1)S(1)}, bf16[128,2048]{1,0:T(8,128)(2,1)S(1)}, u32[]{:S(2)}, u32[]{:S(2)}) collective-permute-start(bf16[128,2048]{1,0:T(8,128)(2,1)S(1)} %get-tuple-element.40), channel_id=1, source_target_pairs={{0,1},{1,0},{2,3},{3,2},{4,5},{5,4},{6,7},{7,6},{8,9},{9,8},{10,11... | collective-permute-start | bytes 1572872 | tf_op jit(solution)/shard_map/ppermute | solution.py:471
  76.6 16.2 %collective-permute-start.28 = (bf16[128,2048]{1,0:T(8,128)(2,1)S(1)}, bf16[128,2048]{1,0:T(8,128)(2,1)S(1)}, u32[]{:S(2)}, u32[]{:S(2)}) collective-permute-start(bf16[128,2048]{1,0:T(8,128)(2,1)S(1)} %get-tuple-element.44), channel_id=1, source_target_pairs={{0,1},{1,0},{2,3},{3,2},{4,5},{5,4},{6,7},{7,6},{8,9},{9,8},{10,11... | collective-permute-start | bytes 1572872 | tf_op jit(solution)/shard_map/ppermute | solution.py:471
  76.7 26.6 %collective-permute-start.9 = (bf16[64,2048]{1,0:T(8,128)(2,1)S(1)}, bf16[64,2048]{1,0:T(8,128)(2,1)S(1)}, u32[]{:S(2)}, u32[]{:S(2)}) collective-permute-start(bf16[64,2048]{1,0:T(8,128)(2,1)S(1)} %add_convert_fusion.8), channel_id=1, source_target_pairs={{0,2},{1,3},{2,0},{3,1},{4,6},{5,7},{6,4},{7,5},{8,10},{9,11},{10,... | collective-permute-start | bytes 786440 | tf_op jit(solution)/shard_map/ppermute | solution.py:471
  77.4 14.2 %collective-permute-start.15 = (bf16[64,2048]{1,0:T(8,128)(2,1)S(1)}, bf16[64,2048]{1,0:T(8,128)(2,1)S(1)}, u32[]{:S(2)}, u32[]{:S(2)}) collective-permute-start(bf16[64,2048]{1,0:T(8,128)(2,1)S(1)} %add_convert_fusion.6), channel_id=1, source_target_pairs={{0,2},{1,3},{2,0},{3,1},{4,6},{5,7},{6,4},{7,5},{8,10},{9,11},{10,... | collective-permute-start | bytes 786440 | tf_op jit(solution)/shard_map/ppermute | solution.py:471
  79.0 18.2 %collective-permute-start.22 = (bf16[64,2048]{1,0:T(8,128)(2,1)S(1)}, bf16[64,2048]{1,0:T(8,128)(2,1)S(1)}, u32[]{:S(2)}, u32[]{:S(2)}) collective-permute-start(bf16[64,2048]{1,0:T(8,128)(2,1)S(1)} %add_convert_fusion.4), channel_id=1, source_target_pairs={{0,2},{1,3},{2,0},{3,1},{4,6},{5,7},{6,4},{7,5},{8,10},{9,11},{10,... | collective-permute-start | bytes 786440 | tf_op jit(solution)/shard_map/ppermute | solution.py:471
  91.7 11.6 %collective-permute-start.16 = (bf16[64,2048]{1,0:T(8,128)(2,1)S(1)}, bf16[64,2048]{1,0:T(8,128)(2,1)S(1)}, u32[]{:S(2)}, u32[]{:S(2)}) collective-permute-start(bf16[64,2048]{1,0:T(8,128)(2,1)S(1)} %add_convert_fusion.5), channel_id=1, source_target_pairs={{0,4},{4,0},{8,12},{12,8},{1,5},{5,1},{9,13},{13,9},{2,6},{6,2},{1... | collective-permute-start | bytes 786440 | tf_op jit(solution)/shard_map/ppermute | solution.py:471
  92.8 9.5 %collective-permute-start.29 = (bf16[64,2048]{1,0:T(8,128)(2,1)S(1)}, bf16[64,2048]{1,0:T(8,128)(2,1)S(1)}, u32[]{:S(2)}, u32[]{:S(2)}) collective-permute-start(bf16[64,2048]{1,0:T(8,128)(2,1)S(1)} %add_convert_fusion.2), channel_id=1, source_target_pairs={{0,2},{1,3},{2,0},{3,1},{4,6},{5,7},{6,4},{7,5},{8,10},{9,11},{10,... | collective-permute-start | bytes 786440 | tf_op jit(solution)/shard_map/ppermute | solution.py:471
  97.3 17.9 %collective-permute-start.23 = (bf16[64,2048]{1,0:T(8,128)(2,1)S(1)}, bf16[64,2048]{1,0:T(8,128)(2,1)S(1)}, u32[]{:S(2)}, u32[]{:S(2)}) collective-permute-start(bf16[64,2048]{1,0:T(8,128)(2,1)S(1)} %add_convert_fusion.3), channel_id=1, source_target_pairs={{0,8},{4,12},{8,0},{12,4},{1,9},{5,13},{9,1},{13,5},{2,10},{6,14},... | collective-permute-start | bytes 786440 | tf_op jit(solution)/shard_map/ppermute | solution.py:471
  102.4 19.6 %collective-permute-start.30 = (bf16[64,2048]{1,0:T(8,128)(2,1)S(1)}, bf16[64,2048]{1,0:T(8,128)(2,1)S(1)}, u32[]{:S(2)}, u32[]{:S(2)}) collective-permute-start(bf16[64,2048]{1,0:T(8,128)(2,1)S(1)} %add_convert_fusion.1), channel_id=1, source_target_pairs={{0,12},{4,8},{8,4},{12,0},{1,13},{5,9},{9,5},{13,1},{2,14},{6,10},... | collective-permute-start | bytes 786440 | tf_op jit(solution)/shard_map/ppermute | solution.py:471
  (18 other events, 247.4 us)
where the time goes:
time: 123 us
  waiting for transfers between devices  71.5 us (58%)
  starting transfers between devices  24.2 us (20%)
  Pallas kernels  21.9 us (18%)
  other arithmetic  2.63 us (2%)
  local copies, waits for them, and re-layouts  2.63 us (2%)
    ppermute x31, waiting for transfers between devices, across(): return lax.ppermute(value, axis, [(i, i ^ step) for i in range(size)])  71.5 us
    ppermute x31, starting transfers between devices, across(): return lax.ppermute(value, axis, [(i, i ^ step) for i in range(size)])  24.2 us
    pallas_call x8, Pallas kernels, on_core(): pl.pallas_call(kernel, out_shape=results, in_specs=[VMEM_SPEC] * len(args...  21.9 us
  transfers between devices with their start and end apart: 31, of which 14 were waited for; matrix products, arithmetic and copies ran while one was open for 1% of the time, Pallas kernels for 15%

commit v1 on v0

--- a/solution.py
+++ b/solution.py
@@ -220,7 +220,7 @@
 WAIT_FLOPS = 8 * 10**9
 
 
-def on_core(kernel, results, args, flops=0, exps=0, vmem=24):
+def on_core(kernel, results, args, flops=0, exps=0, vmem=16):
     moved = sum(a.size * a.dtype.itemsize for a in list(args) + list(results))
     return pl.pallas_call(
         kernel,
@@ -257,17 +257,10 @@
     return lax.rsqrt(jnp.sum(values * values, axis=1, keepdims=True) / width + EPS)
 
 
-def packed(wide_pair, narrow_pair):
-    return jnp.concatenate(
-        [jnp.concatenate(wide_pair, axis=1)] + [a.T for a in narrow_pair], axis=0
-    )
-
-
 def prepare_kernel(
     order,
     own_rows,
-    qw_ref,
-    qn_ref,
+    query_ref,
     small_ref,
     qw_out,
     qn_out,
@@ -302,12 +295,12 @@
         source = pl.ds(pl.multiple_of((tp ^ r) * own_rows, own_rows), own_rows)
         place = pl.ds(pl.multiple_of(sp * count + (tp ^ r) * own_rows, own_rows), own_rows)
         target = pl.ds(slot * own_rows, own_rows)
-        for h in range(qw_ref.shape[1] // lanes):
+        for h in range(qw_out.shape[1] // lanes):
             head = pl.ds(h * lanes, lanes)
-            value = qw_ref[source, head].astype(jnp.float32)
+            value = query_ref[source, head].astype(jnp.float32)
             value = value * rms(value, lanes) * gain_wide
             qw_out[target, head] = rotated(value, lanes // 4, cw_ref[place, :], sw_ref[place, :])
-        value = qn_ref[source, :].astype(jnp.float32)
+        value = query_ref[source, qw_out.shape[1] :].astype(jnp.float32)
         low = lanes_of(value.shape) < lanes // 2
         first = rms(jnp.where(low, value, 0.0), lanes // 2)
         second = rms(jnp.where(low, 0.0, value), lanes // 2)
@@ -332,77 +325,89 @@
     return top, total, mixed
 
 
-def keys_and_values(raw_refs, steps, small_ref, tables):
-    cw_ref, sw_ref, cn_ref, sn_ref = tables
+def wide_keys(raw_refs, steps, small_ref, cos_ref, sin_ref):
     lanes = small_ref.shape[1]
     sp = lax.axis_index("sp")
-    kw, vw, kn, vn = [], [], [], []
+    keys, values = [], []
     for r, ref in zip(steps, raw_refs, strict=True):
-        count = ref.shape[0] - lanes
+        count = ref.shape[0] // 2
         place = pl.ds(pl.multiple_of((sp ^ r) * count, count), count)
-        value = ref[:count, :lanes].astype(jnp.float32)
+        value = ref[:count, :].astype(jnp.float32)
         value = value * rms(value, lanes) * small_ref[2:3, :]
-        kw.append(rotated(value, lanes // 4, cw_ref[place, :], sw_ref[place, :]))
-        vw.append(ref[:count, lanes:])
-        both = ref[count:, :].astype(jnp.float32).T
+        keys.append(rotated(value, lanes // 4, cos_ref[place, :], sin_ref[place, :]))
+        values.append(ref[count:, :])
+    return jnp.concatenate(keys, axis=0), jnp.concatenate(values, axis=0)
+
+
+def narrow_keys(raw_refs, steps, small_ref, cos_ref, sin_ref):
+    lanes = small_ref.shape[1]
+    sp = lax.axis_index("sp")
+    keys, values = [], []
+    for r, ref in zip(steps, raw_refs, strict=True):
+        count = ref.shape[1]
+        place = pl.ds(pl.multiple_of((sp ^ r) * count, count), count)
+        both = ref[...].astype(jnp.float32).T
         low = lanes_of(both.shape) < lanes // 2
         other = pltpu.roll(both, lanes // 2, 1)
         value = jnp.where(low, both, other)
         value = value * rms(jnp.where(low, both, 0.0), lanes // 2) * small_ref[3:4, :]
-        kn.append(rotated(value, lanes // 8, cn_ref[place, :], sn_ref[place, :]))
-        vn.append(jnp.where(low, other, both).astype(jnp.bfloat16))
-    return [jnp.concatenate(v, axis=0) for v in (kw, vw, kn, vn)]
-
-
-def all_heads(qw_ref, qn_ref, keys, lanes, before=None):
-    kw, vw, kn, vn = keys
-    query = qn_ref[...]
+        keys.append(rotated(value, lanes // 8, cos_ref[place, :], sin_ref[place, :]))
+        values.append(jnp.where(low, other, both).astype(jnp.bfloat16))
+    return jnp.concatenate(keys, axis=0), jnp.concatenate(values, axis=0)
+
+
+def wide_queries(ref, lanes):
+    return [ref[:, h * lanes : (h + 1) * lanes] for h in range(ref.shape[1] // lanes)]
+
+
+def narrow_queries(ref, lanes):
+    query = ref[...]
     low = lanes_of(query.shape) < lanes // 2
     nothing = jnp.zeros_like(query)
-    heads = [
-        (qw_ref[:, h * lanes : (h + 1) * lanes], kw, vw, lanes**-0.5)
-        for h in range(qw_ref.shape[1] // lanes)
-    ]
-    heads.append((jnp.where(low, query, nothing), kn, vn, (lanes // 2) ** -0.5))
-    heads.append((jnp.where(low, nothing, query), kn, vn, (lanes // 2) ** -0.5))
-    before = [None] * len(heads) if before is None else before
-    return [mixed_in(*head, old) for head, old in zip(heads, before, strict=True)]
-
-
-def attend_first_kernel(steps, *refs):
+    return [jnp.where(low, query, nothing), jnp.where(low, nothing, query)]
+
+
+WIDE = (wide_keys, wide_queries, 1)
+NARROW = (narrow_keys, narrow_queries, 2)
+
+
+def attend_first_kernel(kind, steps, *refs):
     raw_refs, refs = refs[: len(steps)], refs[len(steps) :]
-    qw_ref, qn_ref, small_ref = refs[:3]
-    stat_ref, mixed_ref = refs[7:]
+    query_ref, small_ref, cos_ref, sin_ref, stat_ref, mixed_ref = refs
     lanes = small_ref.shape[1]
-    keys = keys_and_values(raw_refs, steps, small_ref, refs[3:7])
-    states = all_heads(qw_ref, qn_ref, keys, lanes)
+    keys, values = kind[0](raw_refs, steps, small_ref, cos_ref, sin_ref)
+    scale = (lanes // kind[2]) ** -0.5
     lane = lanes_of(stat_ref.shape)
     stat = jnp.zeros(stat_ref.shape, jnp.float32)
-    for h, (top, total, mixed) in enumerate(states):
+    for h, query in enumerate(kind[1](query_ref, lanes)):
+        top, total, mixed = mixed_in(query, keys, values, scale)
         stat = jnp.where(lane == 2 * h, top, stat)
         stat = jnp.where(lane == 2 * h + 1, total, stat)
         mixed_ref[h] = mixed
     stat_ref[...] = stat
 
 
-def attend_last_kernel(steps, *refs):
+def attend_last_kernel(kind, steps, *refs):
     raw_refs, refs = refs[: len(steps)], refs[len(steps) :]
-    qw_ref, qn_ref, small_ref = refs[:3]
-    stat_ref, mixed_ref, ow_ref, on_ref, keep_ref, send_ref = refs[7:]
+    query_ref, small_ref, cos_ref, sin_ref, stat_ref, mixed_ref, proj_ref, *refs = refs
     lanes = small_ref.shape[1]
-    keys = keys_and_values(raw_refs, steps, small_ref, refs[3:7])
-    before = [
-        (stat_ref[:, 2 * h : 2 * h + 1], stat_ref[:, 2 * h + 1 : 2 * h + 2], mixed_ref[h])
-        for h in range(mixed_ref.shape[0])
-    ]
-    states = all_heads(qw_ref, qn_ref, keys, lanes, before)
-    heads = [mixed / total for _, total, mixed in states]
-    low = lanes_of(heads[-1].shape) < lanes // 2
-    narrow = jnp.where(low, heads[-2], heads[-1]).astype(jnp.bfloat16)
-    wide = jnp.concatenate(heads[:-2], axis=1).astype(jnp.bfloat16)
-    terms = jnp.dot(wide, ow_ref[...], preferred_element_type=jnp.float32)
-    terms = terms + jnp.dot(narrow, on_ref[...], preferred_element_type=jnp.float32)
-    terms = terms.astype(jnp.bfloat16)
+    keys, values = kind[0](raw_refs, steps, small_ref, cos_ref, sin_ref)
+    scale = (lanes // kind[2]) ** -0.5
+    heads = []
+    for h, query in enumerate(kind[1](query_ref, lanes)):
+        before = (stat_ref[:, 2 * h : 2 * h + 1], stat_ref[:, 2 * h + 1 : 2 * h + 2], mixed_ref[h])
+        _, total, mixed = mixed_in(query, keys, values, scale, before)
+        heads.append(mixed / total)
+    if kind[2] == 1:
+        joined = jnp.concatenate(heads, axis=1)
+    else:
+        joined = jnp.where(lanes_of(heads[0].shape) < lanes // 2, heads[0], heads[1])
+    terms = jnp.dot(joined.astype(jnp.bfloat16), proj_ref[...], preferred_element_type=jnp.float32)
+    if len(refs) == 1:
+        refs[0][...] = terms
+        return
+    terms_ref, keep_ref, send_ref = refs
+    terms = (terms_ref[...] + terms).astype(jnp.bfloat16)
     half = terms.shape[0] // 2
     keep_ref[...] = terms[:half]
     send_ref[...] = terms[half:]
@@ -475,7 +480,14 @@
         one = across(own, "sp", 1)
         return [own, one, two, across(two, "sp", 1)]
 
-    raw_blocks = spread(packed([keys_wide, values_wide], [keys_narrow, values_narrow]))
+    def joined(first, second, axis):
+        least = jnp.array(-jnp.inf, first.dtype)
+        after, before = [(0, 0, 0)] * 2, [(0, 0, 0)] * 2
+        after[axis], before[axis] = (0, second.shape[axis], 0), (first.shape[axis], 0, 0)
+        return jnp.maximum(lax.pad(first, least, after), lax.pad(second, least, before))
+
+    raw_wide = spread(joined(keys_wide, values_wide, 0))
+    raw_narrow = spread(jnp.concatenate([keys_narrow.T, values_narrow.T], axis=0))
 
     table = like(tokens, lanes, jnp.float32)
     small = jnp.concatenate(
@@ -486,28 +498,44 @@
     q_wide, q_narrow, *tables = on_core(
         functools.partial(prepare_kernel, order, own_rows),
         [like(*queries_wide.shape), like(*queries_narrow.shape)] + [table] * 4,
-        [queries_wide, queries_narrow, small],
+        [joined(queries_wide, queries_narrow, 1), small],
         flops=WAIT_FLOPS,
     )
-    heads = queries_wide.shape[1] // lanes + queries_narrow.shape[1] // (lanes // 2)
-    shared = [q_wide, q_narrow, small] + tables
-    one_block = dict(flops=WAIT_FLOPS, exps=heads * tok_count**2)
-    stat, mixed = on_core(
-        functools.partial(attend_first_kernel, (0, 1, 2)),
-        [
-            like(tok_count, lanes, jnp.float32),
-            jax.ShapeDtypeStruct((heads, tok_count, lanes), jnp.float32),
-        ],
-        raw_blocks[:3] + shared,
-        **one_block,
-    )
-    keep, send = on_core(
-        functools.partial(attend_last_kernel, (3,)),
-        [like(half, model_width)] * 2,
-        raw_blocks[3:] + shared + [stat, mixed, output_wide, output_narrow],
-        **one_block,
-    )
+    near, far = tuple(range(n_sp - 1)), (n_sp - 1,)
+    parts = {
+        "wide": (WIDE, raw_wide, [q_wide, small] + tables[:2], output_wide),
+        "narrow": (NARROW, raw_narrow, [q_narrow, small] + tables[2:], output_narrow),
+    }
+    cost = dict(flops=WAIT_FLOPS // 2, exps=4 * tok_count**2)
+    states = {}
+    for name, (kind, raw, shared, _) in parts.items():
+        heads = shared[0].shape[1] // lanes * kind[2]
+        states[name] = on_core(
+            functools.partial(attend_first_kernel, kind, near),
+            [
+                like(tok_count, lanes, jnp.float32),
+                jax.ShapeDtypeStruct((heads, tok_count, lanes), jnp.float32),
+            ],
+            raw[:-1] + shared,
+            **cost,
+        )
+    outs, terms = [like(tok_count, model_width, jnp.float32)], []
+    for name, (kind, raw, shared, proj) in parts.items():
+        terms = on_core(
+            functools.partial(attend_last_kernel, kind, far),
+            outs,
+            [*raw[-1:], *shared, *states[name], proj, *terms],
+            **cost,
+        )
+        outs = [like(half, model_width)] * 2
+    keep, send = terms
     came = across(send, "tp", 1)
+
+    experts = sp ^ jnp.arange(n_sp, dtype=route_ids.dtype)
+    chosen = route_ids[:, :, None] == experts[None, None, :]
+    own_weights = jnp.sum(jnp.where(chosen, route_weights[:, :, None], 0.0), axis=1)
+    own_weights = lax.optimization_barrier((own_weights, send))[0]
+    pair_weights = jnp.concatenate([own_weights, across(own_weights, "tp", 2)], axis=0)
 
     def crossing(keep, came):
         pair = keep[own_rows:].astype(jnp.float32) + came[own_rows:].astype(jnp.float32)
@@ -517,11 +545,11 @@
         norm_kernel,
         [like(own_rows, model_width)] * 2,
         [residual, keep, came, crossing(keep, came), norm_gain[None, :]],
-    )
-
-    total = attended.astype(jnp.float32)
+        flops=WAIT_FLOPS,
+    )
+
     arrived = spread(normed)
-    crossed_rows = []
+    crossed_rows, keeps, cames = [], [], []
     for r in range(n_sp):
         if r % 2:
             crossed_rows.append(across(crossed_rows[r - 1], "sp", 1))
@@ -535,15 +563,29 @@
             rows + [gate_weight, up_weight, down_weight],
             flops=6 * tok_count * model_width * hidden_width,
             exps=tok_count * hidden_width,
+            vmem=12,
         )
-        came = across(send, "tp", 1)
-        crossed = crossing(keep, came).astype(jnp.float32)
-        expert_out = keep[:own_rows].astype(jnp.float32) + came[:own_rows].astype(jnp.float32)
-        expert_out = (expert_out + crossed).astype(jnp.bfloat16)
-        if r:
-            expert_out = across(expert_out, "sp", r)
-        weight = jnp.sum(jnp.where(route_ids == (sp ^ r), route_weights, 0.0), axis=1)
-        total = total + weight[:, None] * expert_out.astype(jnp.float32)
+        keeps.append(keep)
+        cames.append(across(send, "tp", 1))
+
+    def over_cores(r, rows=slice(None)):
+        return keeps[r][rows].astype(jnp.float32) + cames[r][rows].astype(jnp.float32)
+
+    beside = across(over_cores(1).astype(jnp.bfloat16), "sp", 1)
+    gates, far_outs = [], []
+    for r in range(2, n_sp):
+        theirs = over_cores(r, slice(own_rows, None)).astype(jnp.bfloat16)
+        crossed = across(theirs, "tp", 2).astype(jnp.float32)
+        expert_out = (over_cores(r, slice(own_rows)) + crossed).astype(jnp.bfloat16)
+        gates += [theirs] if far_outs else [theirs, expert_out]
+        far_outs.append(across(expert_out, "sp", r).astype(jnp.float32))
+
+    beside = lax.optimization_barrier((beside, *gates))[0].astype(jnp.float32)
+    near_sum = over_cores(0) * pair_weights[:, 0:1] + beside * pair_weights[:, 1:2]
+    crossed = across(near_sum[own_rows:].astype(jnp.bfloat16), "tp", 2)
+    total = attended.astype(jnp.float32) + near_sum[:own_rows] + crossed.astype(jnp.float32)
+    for r, expert_out in enumerate(far_outs, 2):
+        total = total + pair_weights[:own_rows, r : r + 1] * expert_out
     return total.astype(jnp.bfloat16)
 
 

time: 123 us -> 119 us (0.967)
  the two profiles are of different devices: /device:TPU:8 before, /device:TPU:0 now
where the time goes in v1:
time: 119 us; the launch traced here: 117 us
  waiting for transfers between devices  57.2 us (48%)
  starting transfers between devices  25.7 us (22%)
  Pallas kernels  22.8 us (19%)
  local copies, waits for them, and re-layouts  7.04 us (6%)
  other arithmetic  4.48 us (4%)
    ppermute x34, waiting for transfers between devices, across(): return lax.ppermute(value, axis, [(i, i ^ step) for i in range(size)])  57.2 us
    ppermute x34, starting transfers between devices, across(): return lax.ppermute(value, axis, [(i, i ^ step) for i in range(size)])  25.7 us
    pallas_call x10, Pallas kernels, on_core(): pl.pallas_call(kernel, out_shape=results, in_specs=[VMEM_SPEC] * len(args...  22.8 us
    unnamed x24, local copies, waits for them, and re-layouts  6.15 us
  transfers between devices with their start and end apart: 34, of which 12 were waited for; matrix products, arithmetic and copies ran while one was open for 3% of the time, Pallas kernels for 17%

profile of v1, /device:TPU:0, one launch (start us, length us, event | category | flops | bytes accessed | tf_op | source)
XLA Modules:
  0.0 117.5 jit_solution(17744775973583309412)
XLA Ops:
  0.9 4.1 %collective-permute-start.3 = (bf16[512,128]{1,0:T(8,128)(2,1)S(1)}, bf16[512,128]{1,0:T(8,128)(2,1)S(1)}, u32[]{:S(2)}, u32[]{:S(2)}) collective-permute-start(bf16[512,128]{1,0:T(8,128)(2,1)S(1)} %pad_maximum_fusion.1.refs_0_), channel_id=1, source_target_pairs={{0,8},{4,12},{8,0},{12,4},{1,9},{5,13},{9,1},{13,5},{2,10},{6,14},... | collective-permute-start | bytes 393224 | tf_op jit(solution)/shard_map/ppermute | solution.py:476
  11.2 2.3 %collective-permute-done.refs_2_ = bf16[128,256]{1,0:T(8,128)(2,1)S(1)} collective-permute-done((bf16[128,256]{1,0:T(8,128)(2,1)S(1)}, bf16[128,256]{1,0:T(8,128)(2,1)S(1)}, u32[]{:S(2)}, u32[]{:S(2)}) %collective-permute-start) | collective-permute-done | bytes 65568 | tf_op jit(solution)/shard_map/ppermute | solution.py:476
  15.1 1.8 %shard_map.200 = (f32[256,128]{1,0:T(8,128)S(1)}, f32[2,256,128]{2,1,0:T(8,128)S(1)}) custom-call(bf16[128,256]{1,0:T(8,128)(2,1)S(1)} %pad_maximum_fusion.2.refs_0_, bf16[128,256]{1,0:T(8,128)(2,1)S(1)} %collective-permute-done.2.refs_1_, bf16[128,256]{1,0:T(8,128)(2,1)S(1)} %collective-permute-done.refs_2_, ...), custom_call_target="tpu_custom_call" | custom-call | flops 4000000000 | bytes 1707008 | tf_op jit(solution)/shard_map/pallas_call | solution.py:225
  19.3 2.7 %collective-permute-done.4.refs_0_ = bf16[512,128]{1,0:T(8,128)(2,1)S(1)} collective-permute-done((bf16[512,128]{1,0:T(8,128)(2,1)S(1)}, bf16[512,128]{1,0:T(8,128)(2,1)S(1)}, u32[]{:S(2)}, u32[]{:S(2)}) %collective-permute-start.4) | collective-permute-done | bytes 131104 | tf_op jit(solution)/shard_map/ppermute | solution.py:476
  22.0 1.7 %shard_map.202.refs_8_ = f32[256,2048]{1,0:T(8,128)S(1)} custom-call(bf16[512,128]{1,0:T(8,128)(2,1)S(1)} %collective-permute-done.4.refs_0_, bf16[256,256]{1,0:T(8,128)(2,1)S(1)} %get-tuple-element.34.refs_3_.refs_1_, f32[6,128]{1,0:T(8,128)S(1)} %bitcast.15, f32[1024,128]{1,0:T(8,128)S(1)} %get-tuple-element.35.refs_5_.refs_3_, ...), custom_call_target="tpu_custom_call" | custom-call | flops 4000000000 | bytes 4852736 | tf_op jit(solution)/shard_map/pallas_call | solution.py:225
  23.8 2.0 %shard_map.203 = (bf16[128,2048]{1,0:T(8,128)(2,1)S(1)}, bf16[128,2048]{1,0:T(8,128)(2,1)S(1)}) custom-call(bf16[128,256]{1,0:T(8,128)(2,1)S(1)} %collective-permute-done.1.refs_0_, bf16[256,128]{1,0:T(8,128)(2,1)S(1)} %get-tuple-element.29.refs_3_.refs_1_, f32[6,128]{1,0:T(8,128)S(1)} %bitcast.16, f32[1024,128]{1,0:T(8,128)S(1)} %get-tuple-element.30.refs_5_.refs_3_, ...), custom_call_target="tpu_custom_call" | custom-call | flops 4000000000 | bytes 5245952 | tf_op jit(solution)/shard_map/pallas_call | solution.py:225
  25.9 1.9 %collective-permute-done.6.came_ref = bf16[128,2048]{1,0:T(8,128)(2,1)S(1)} collective-permute-done((bf16[128,2048]{1,0:T(8,128)(2,1)S(1)}, bf16[128,2048]{1,0:T(8,128)(2,1)S(1)}, u32[]{:S(2)}, u32[]{:S(2)}) %collective-permute-start.6) | collective-permute-done | bytes 524320 | tf_op jit(solution)/shard_map/ppermute | solution.py:476
  29.4 6.9 %collective-permute-done.7.crossed_ref = bf16[64,2048]{1,0:T(8,128)(2,1)S(1)} collective-permute-done((bf16[64,2048]{1,0:T(8,128)(2,1)S(1)}, bf16[64,2048]{1,0:T(8,128)(2,1)S(1)}, u32[]{:S(2)}, u32[]{:S(2)}) %collective-permute-start.7) | collective-permute-done | bytes 262176 | tf_op jit(solution)/shard_map/ppermute | solution.py:476
  36.6 3.4 %collective-permute-start.19 = (bf16[64,2048]{1,0:T(8,128)(2,1)S(1)}, bf16[64,2048]{1,0:T(8,128)(2,1)S(1)}, u32[]{:S(2)}, u32[]{:S(2)}) collective-permute-start(bf16[64,2048]{1,0:T(8,128)(2,1)S(1)} %get-tuple-element.42.r0_ref), channel_id=1, source_target_pairs={{0,8},{4,12},{8,0},{12,4},{1,9},{5,13},{9,1},{13,5},{2,10},{6,14},... | collective-permute-start | bytes 786440 | tf_op jit(solution)/shard_map/ppermute | solution.py:476
  42.4 8.8 %collective-permute-done.19.r0_ref = bf16[64,2048]{1,0:T(8,128)(2,1)S(1)} collective-permute-done((bf16[64,2048]{1,0:T(8,128)(2,1)S(1)}, bf16[64,2048]{1,0:T(8,128)(2,1)S(1)}, u32[]{:S(2)}, u32[]{:S(2)}) %collective-permute-start.19) | collective-permute-done | bytes 262176 | tf_op jit(solution)/shard_map/ppermute | solution.py:476
  53.3 3.0 %collective-permute-done.13.r0_ref = bf16[64,2048]{1,0:T(8,128)(2,1)S(1)} collective-permute-done((bf16[64,2048]{1,0:T(8,128)(2,1)S(1)}, bf16[64,2048]{1,0:T(8,128)(2,1)S(1)}, u32[]{:S(2)}, u32[]{:S(2)}) %collective-permute-start.13) | collective-permute-done | bytes 262176 | tf_op jit(solution)/shard_map/ppermute | solution.py:476
  56.4 3.0 %collective-permute-done.20.r2_ref = bf16[64,2048]{1,0:T(8,128)(2,1)S(1)} collective-permute-done((bf16[64,2048]{1,0:T(8,128)(2,1)S(1)}, bf16[64,2048]{1,0:T(8,128)(2,1)S(1)}, u32[]{:S(2)}, u32[]{:S(2)}) %collective-permute-start.20) | collective-permute-done | bytes 262176 | tf_op jit(solution)/shard_map/ppermute | solution.py:476
  59.8 2.0 %copy-done = bf16[1,2048,896]{2,1,0:T(8,128)(2,1)S(1)} copy-done((bf16[1,2048,896]{2,1,0:T(8,128)(2,1)S(1)}, bf16[1,2048,896]{2,1,0:T(8,128)(2,1)}, u32[]{:S(2)}) %copy-start) | copy-done | bytes 3670040
  61.9 2.0 %copy-done.2 = bf16[1,2048,896]{2,1,0:T(8,128)(2,1)S(1)} copy-done((bf16[1,2048,896]{2,1,0:T(8,128)(2,1)S(1)}, bf16[1,2048,896]{2,1,0:T(8,128)(2,1)}, u32[]{:S(2)}) %copy-start.2) | copy-done | bytes 3670040
  63.9 2.0 %copy-done.4 = bf16[1,896,2048]{2,1,0:T(8,128)(2,1)S(1)} copy-done((bf16[1,896,2048]{2,1,0:T(8,128)(2,1)S(1)}, bf16[1,896,2048]{2,1,0:T(8,128)(2,1)}, u32[]{:S(2)}) %copy-start.4) | copy-done | bytes 3670040
  66.0 3.4 %shard_map.205 = (bf16[128,2048]{1,0:T(8,128)(2,1)S(1)}, bf16[128,2048]{1,0:T(8,128)(2,1)S(1)}) custom-call(bf16[64,2048]{1,0:T(8,128)(2,1)S(1)} %get-tuple-element.42.r0_ref, bf16[64,2048]{1,0:T(8,128)(2,1)S(1)} %collective-permute-done.8.r2_ref, bf16[64,2048]{1,0:T(8,128)(2,1)S(1)} %collective-permute-done.9.r1_ref, ...), custom_call_target="tpu_custom_call" | custom-call | flops 2818572288 | bytes 13107200 | tf_op jit(solution)/shard_map/pallas_call | solution.py:225
  70.2 3.6 %shard_map.207 = (bf16[128,2048]{1,0:T(8,128)(2,1)S(1)}, bf16[128,2048]{1,0:T(8,128)(2,1)S(1)}) custom-call(bf16[64,2048]{1,0:T(8,128)(2,1)S(1)} %collective-permute-done.19.r0_ref, bf16[64,2048]{1,0:T(8,128)(2,1)S(1)} %collective-permute-done.20.r2_ref, bf16[64,2048]{1,0:T(8,128)(2,1)S(1)} %collective-permute-done.21.r1_ref, ...), custom_call_target="tpu_custom_call" | custom-call | flops 2818572288 | bytes 13107200 | tf_op jit(solution)/shard_map/pallas_call | solution.py:225
  74.3 3.9 %collective-permute-done.26.r2_ref = bf16[64,2048]{1,0:T(8,128)(2,1)S(1)} collective-permute-done((bf16[64,2048]{1,0:T(8,128)(2,1)S(1)}, bf16[64,2048]{1,0:T(8,128)(2,1)S(1)}, u32[]{:S(2)}, u32[]{:S(2)}) %collective-permute-start.26) | collective-permute-done | bytes 262176 | tf_op jit(solution)/shard_map/ppermute | solution.py:476
  78.2 3.4 %shard_map.206 = (bf16[128,2048]{1,0:T(8,128)(2,1)S(1)}, bf16[128,2048]{1,0:T(8,128)(2,1)S(1)}) custom-call(bf16[64,2048]{1,0:T(8,128)(2,1)S(1)} %collective-permute-done.13.r0_ref, bf16[64,2048]{1,0:T(8,128)(2,1)S(1)} %collective-permute-done.14.r2_ref, bf16[64,2048]{1,0:T(8,128)(2,1)S(1)} %collective-permute-done.15.r1_ref, ...), custom_call_target="tpu_custom_call" | custom-call | flops 2818572288 | bytes 13107200 | tf_op jit(solution)/shard_map/pallas_call | solution.py:225
  82.2 3.4 %shard_map.208 = (bf16[128,2048]{1,0:T(8,128)(2,1)S(1)}, bf16[128,2048]{1,0:T(8,128)(2,1)S(1)}) custom-call(bf16[64,2048]{1,0:T(8,128)(2,1)S(1)} %collective-permute-done.25.r0_ref, bf16[64,2048]{1,0:T(8,128)(2,1)S(1)} %collective-permute-done.26.r2_ref, bf16[64,2048]{1,0:T(8,128)(2,1)S(1)} %collective-permute-done.27.r1_ref, ...), custom_call_target="tpu_custom_call" | custom-call | flops 2818572288 | bytes 13107200 | tf_op jit(solution)/shard_map/pallas_call | solution.py:225
  89.3 5.8 %collective-permute-done.24 = bf16[64,2048]{1,0:T(8,128)(2,1)S(1)} collective-permute-done((bf16[64,2048]{1,0:T(8,128)(2,1)S(1)}, bf16[64,2048]{1,0:T(8,128)(2,1)S(1)}, u32[]{:S(2)}, u32[]{:S(2)}) %collective-permute-start.24) | collective-permute-done | bytes 262176 | tf_op jit(solution)/shard_map/ppermute | solution.py:476
  95.5 4.7 %collective-permute-done.32 = bf16[64,2048]{1,0:T(8,128)(2,1)S(1)} collective-permute-done((bf16[64,2048]{1,0:T(8,128)(2,1)S(1)}, bf16[64,2048]{1,0:T(8,128)(2,1)S(1)}, u32[]{:S(2)}, u32[]{:S(2)}) %collective-permute-start.32) | collective-permute-done | bytes 262176 | tf_op jit(solution)/shard_map/ppermute | solution.py:476
  101.8 3.3 %collective-permute-done.18 = bf16[128,2048]{1,0:T(8,128)(2,1)S(1)} collective-permute-done((bf16[128,2048]{1,0:T(8,128)(2,1)S(1)}, bf16[128,2048]{1,0:T(8,128)(2,1)S(1)}, u32[]{:S(2)}, u32[]{:S(2)}) %collective-permute-start.18) | collective-permute-done | bytes 524320 | tf_op jit(solution)/shard_map/ppermute | solution.py:476
  105.5 11.0 %collective-permute-done.31 = bf16[64,2048]{1,0:T(8,128)(2,1)S(1)} collective-permute-done((bf16[64,2048]{1,0:T(8,128)(2,1)S(1)}, bf16[64,2048]{1,0:T(8,128)(2,1)S(1)}, u32[]{:S(2)}, u32[]{:S(2)}) %collective-permute-start.31) | collective-permute-done | bytes 262176 | tf_op jit(solution)/shard_map/ppermute | solution.py:476
  (96 shorter events, 26.9 us)
Async XLA Ops:
  0.9 16.1 %collective-permute-start.3 = (bf16[512,128]{1,0:T(8,128)(2,1)S(1)}, bf16[512,128]{1,0:T(8,128)(2,1)S(1)}, u32[]{:S(2)}, u32[]{:S(2)}) collective-permute-start(bf16[512,128]{1,0:T(8,128)(2,1)S(1)} %pad_maximum_fusion.1.refs_0_), channel_id=1, source_target_pairs={{0,8},{4,12},{8,0},{12,4},{1,9},{5,13},{9,1},{13,5},{2,10},{6,14},... | collective-permute-start | bytes 393224 | tf_op jit(solution)/shard_map/ppermute | solution.py:476
  5.0 12.8 %collective-permute-start.5 = (bf16[512,128]{1,0:T(8,128)(2,1)S(1)}, bf16[512,128]{1,0:T(8,128)(2,1)S(1)}, u32[]{:S(2)}, u32[]{:S(2)}) collective-permute-start(bf16[512,128]{1,0:T(8,128)(2,1)S(1)} %pad_maximum_fusion.1.refs_0_), channel_id=1, source_target_pairs={{0,4},{4,0},{8,12},{12,8},{1,5},{5,1},{9,13},{13,9},{2,6},{6,2},{1... | collective-permute-start | bytes 393224 | tf_op jit(solution)/shard_map/ppermute | solution.py:476
  13.4 10.3 %collective-permute-start.1 = (bf16[128,256]{1,0:T(8,128)(2,1)S(1)}, bf16[128,256]{1,0:T(8,128)(2,1)S(1)}, u32[]{:S(2)}, u32[]{:S(2)}) collective-permute-start(bf16[128,256]{1,0:T(8,128)(2,1)S(1)} %collective-permute-done.refs_2_), channel_id=1, source_target_pairs={{0,4},{4,0},{8,12},{12,8},{1,5},{5,1},{9,13},{13,9},{2,6},{6,2},{1... | collective-permute-start | bytes 196616 | tf_op jit(solution)/shard_map/ppermute | solution.py:476
  27.9 8.4 %collective-permute-start.7 = (bf16[64,2048]{1,0:T(8,128)(2,1)S(1)}, bf16[64,2048]{1,0:T(8,128)(2,1)S(1)}, u32[]{:S(2)}, u32[]{:S(2)}) collective-permute-start(bf16[64,2048]{1,0:T(8,128)(2,1)S(1)} %add_convert_fusion.5), channel_id=1, source_target_pairs={{0,2},{1,3},{2,0},{3,1},{4,6},{5,7},{6,4},{7,5},{8,10},{9,11},{10,... | collective-permute-start | bytes 786440 | tf_op jit(solution)/shard_map/ppermute | solution.py:476
  36.6 14.6 %collective-permute-start.19 = (bf16[64,2048]{1,0:T(8,128)(2,1)S(1)}, bf16[64,2048]{1,0:T(8,128)(2,1)S(1)}, u32[]{:S(2)}, u32[]{:S(2)}) collective-permute-start(bf16[64,2048]{1,0:T(8,128)(2,1)S(1)} %get-tuple-element.42.r0_ref), channel_id=1, source_target_pairs={{0,8},{4,12},{8,0},{12,4},{1,9},{5,13},{9,1},{13,5},{2,10},{6,14},... | collective-permute-start | bytes 786440 | tf_op jit(solution)/shard_map/ppermute | solution.py:476
  40.0 12.7 %collective-permute-start.8 = (bf16[64,2048]{1,0:T(8,128)(2,1)S(1)}, bf16[64,2048]{1,0:T(8,128)(2,1)S(1)}, u32[]{:S(2)}, u32[]{:S(2)}) collective-permute-start(bf16[64,2048]{1,0:T(8,128)(2,1)S(1)} %get-tuple-element.42.r0_ref), channel_id=1, source_target_pairs={{0,2},{1,3},{2,0},{3,1},{4,6},{5,7},{6,4},{7,5},{8,10},{9,11},{10,... | collective-permute-start | bytes 786440 | tf_op jit(solution)/shard_map/ppermute | solution.py:476
  41.5 11.1 %collective-permute-start.12 = (f32[64,4]{0,1:T(4,128)S(1)}, f32[64,4]{0,1:T(4,128)S(1)}, u32[]{:S(2)}, u32[]{:S(2)}) collective-permute-start(f32[64,4]{0,1:T(4,128)S(1)} %select_reduce_fusion), channel_id=1, source_target_pairs={{0,2},{1,3},{2,0},{3,1},{4,6},{5,7},{6,4},{7,5},{8,10},{9,11},{10,... | collective-permute-start | bytes 3080 | tf_op jit(solution)/shard_map/ppermute | solution.py:476
  42.1 10.7 %collective-permute-start.9 = (bf16[64,2048]{1,0:T(8,128)(2,1)S(1)}, bf16[64,2048]{1,0:T(8,128)(2,1)S(1)}, u32[]{:S(2)}, u32[]{:S(2)}) collective-permute-start(bf16[64,2048]{1,0:T(8,128)(2,1)S(1)} %get-tuple-element.42.r0_ref), channel_id=1, source_target_pairs={{0,1},{1,0},{2,3},{3,2},{4,5},{5,4},{6,7},{7,6},{8,9},{9,8},{10,11... | collective-permute-start | bytes 786440 | tf_op jit(solution)/shard_map/ppermute | solution.py:476
  42.1 14.3 %collective-permute-start.13 = (bf16[64,2048]{1,0:T(8,128)(2,1)S(1)}, bf16[64,2048]{1,0:T(8,128)(2,1)S(1)}, u32[]{:S(2)}, u32[]{:S(2)}) collective-permute-start(bf16[64,2048]{1,0:T(8,128)(2,1)S(1)} %get-tuple-element.42.r0_ref), channel_id=1, source_target_pairs={{0,4},{4,0},{8,12},{12,8},{1,5},{5,1},{9,13},{13,9},{2,6},{6,2},{1... | collective-permute-start | bytes 786440 | tf_op jit(solution)/shard_map/ppermute | solution.py:476
  52.7 16.7 %collective-permute-start.25 = (bf16[64,2048]{1,0:T(8,128)(2,1)S(1)}, bf16[64,2048]{1,0:T(8,128)(2,1)S(1)}, u32[]{:S(2)}, u32[]{:S(2)}) collective-permute-start(bf16[64,2048]{1,0:T(8,128)(2,1)S(1)} %collective-permute-done.19.r0_ref), channel_id=1, source_target_pairs={{0,4},{4,0},{8,12},{12,8},{1,5},{5,1},{9,13},{13,9},{2,6},{6,2},{1... | collective-permute-start | bytes 786440 | tf_op jit(solution)/shard_map/ppermute | solution.py:476
  52.8 16.7 %collective-permute-start.21 = (bf16[64,2048]{1,0:T(8,128)(2,1)S(1)}, bf16[64,2048]{1,0:T(8,128)(2,1)S(1)}, u32[]{:S(2)}, u32[]{:S(2)}) collective-permute-start(bf16[64,2048]{1,0:T(8,128)(2,1)S(1)} %collective-permute-done.19.r0_ref), channel_id=1, source_target_pairs={{0,1},{1,0},{2,3},{3,2},{4,5},{5,4},{6,7},{7,6},{8,9},{9,8},{10,11... | collective-permute-start | bytes 786440 | tf_op jit(solution)/shard_map/ppermute | solution.py:476
  56.4 13.2 %collective-permute-start.14 = (bf16[64,2048]{1,0:T(8,128)(2,1)S(1)}, bf16[64,2048]{1,0:T(8,128)(2,1)S(1)}, u32[]{:S(2)}, u32[]{:S(2)}) collective-permute-start(bf16[64,2048]{1,0:T(8,128)(2,1)S(1)} %collective-permute-done.8.r2_ref), channel_id=1, source_target_pairs={{0,4},{4,0},{8,12},{12,8},{1,5},{5,1},{9,13},{13,9},{2,6},{6,2},{1... | collective-permute-start | bytes 786440 | tf_op jit(solution)/shard_map/ppermute | solution.py:476
  59.3 14.5 %collective-permute-start.15 = (bf16[64,2048]{1,0:T(8,128)(2,1)S(1)}, bf16[64,2048]{1,0:T(8,128)(2,1)S(1)}, u32[]{:S(2)}, u32[]{:S(2)}) collective-permute-start(bf16[64,2048]{1,0:T(8,128)(2,1)S(1)} %collective-permute-done.13.r0_ref), channel_id=1, source_target_pairs={{0,1},{1,0},{2,3},{3,2},{4,5},{5,4},{6,7},{7,6},{8,9},{9,8},{10,11... | collective-permute-start | bytes 786440 | tf_op jit(solution)/shard_map/ppermute | solution.py:476
  59.3 10.7 %collective-permute-start.22 = (bf16[64,2048]{1,0:T(8,128)(2,1)S(1)}, bf16[64,2048]{1,0:T(8,128)(2,1)S(1)}, u32[]{:S(2)}, u32[]{:S(2)}) collective-permute-start(bf16[64,2048]{1,0:T(8,128)(2,1)S(1)} %collective-permute-done.20.r2_ref), channel_id=1, source_target_pairs={{0,1},{1,0},{2,3},{3,2},{4,5},{5,4},{6,7},{7,6},{8,9},{9,8},{10,11... | collective-permute-start | bytes 786440 | tf_op jit(solution)/shard_map/ppermute | solution.py:476
  69.4 35.7 %collective-permute-start.11 = (bf16[128,2048]{1,0:T(8,128)(2,1)S(1)}, bf16[128,2048]{1,0:T(8,128)(2,1)S(1)}, u32[]{:S(2)}, u32[]{:S(2)}) collective-permute-start(bf16[128,2048]{1,0:T(8,128)(2,1)S(1)} %get-tuple-element.44), channel_id=1, source_target_pairs={{0,1},{1,0},{2,3},{3,2},{4,5},{5,4},{6,7},{7,6},{8,9},{9,8},{10,11... | collective-permute-start | bytes 1572872 | tf_op jit(solution)/shard_map/ppermute | solution.py:476
  69.5 8.7 %collective-permute-start.26 = (bf16[64,2048]{1,0:T(8,128)(2,1)S(1)}, bf16[64,2048]{1,0:T(8,128)(2,1)S(1)}, u32[]{:S(2)}, u32[]{:S(2)}) collective-permute-start(bf16[64,2048]{1,0:T(8,128)(2,1)S(1)} %collective-permute-done.20.r2_ref), channel_id=1, source_target_pairs={{0,4},{4,0},{8,12},{12,8},{1,5},{5,1},{9,13},{13,9},{2,6},{6,2},{1... | collective-permute-start | bytes 786440 | tf_op jit(solution)/shard_map/ppermute | solution.py:476
  69.6 12.6 %collective-permute-start.27 = (bf16[64,2048]{1,0:T(8,128)(2,1)S(1)}, bf16[64,2048]{1,0:T(8,128)(2,1)S(1)}, u32[]{:S(2)}, u32[]{:S(2)}) collective-permute-start(bf16[64,2048]{1,0:T(8,128)(2,1)S(1)} %collective-permute-done.25.r0_ref), channel_id=1, source_target_pairs={{0,1},{1,0},{2,3},{3,2},{4,5},{5,4},{6,7},{7,6},{8,9},{9,8},{10,11... | collective-permute-start | bytes 786440 | tf_op jit(solution)/shard_map/ppermute | solution.py:476
  73.8 11.9 %collective-permute-start.23 = (bf16[128,2048]{1,0:T(8,128)(2,1)S(1)}, bf16[128,2048]{1,0:T(8,128)(2,1)S(1)}, u32[]{:S(2)}, u32[]{:S(2)}) collective-permute-start(bf16[128,2048]{1,0:T(8,128)(2,1)S(1)} %get-tuple-element.49), channel_id=1, source_target_pairs={{0,1},{1,0},{2,3},{3,2},{4,5},{5,4},{6,7},{7,6},{8,9},{9,8},{10,11... | collective-permute-start | bytes 1572872 | tf_op jit(solution)/shard_map/ppermute | solution.py:476
  85.8 9.2 %collective-permute-start.24 = (bf16[64,2048]{1,0:T(8,128)(2,1)S(1)}, bf16[64,2048]{1,0:T(8,128)(2,1)S(1)}, u32[]{:S(2)}, u32[]{:S(2)}) collective-permute-start(bf16[64,2048]{1,0:T(8,128)(2,1)S(1)} %add_convert_fusion.4), channel_id=1, source_target_pairs={{0,2},{1,3},{2,0},{3,1},{4,6},{5,7},{6,4},{7,5},{8,10},{9,11},{10,... | collective-permute-start | bytes 786440 | tf_op jit(solution)/shard_map/ppermute | solution.py:476
  87.5 17.6 %collective-permute-start.18 = (bf16[128,2048]{1,0:T(8,128)(2,1)S(1)}, bf16[128,2048]{1,0:T(8,128)(2,1)S(1)}, u32[]{:S(2)}, u32[]{:S(2)}) collective-permute-start(bf16[128,2048]{1,0:T(8,128)(2,1)S(1)} %add_convert_fusion), channel_id=1, source_target_pairs={{0,4},{4,0},{8,12},{12,8},{1,5},{5,1},{9,13},{13,9},{2,6},{6,2},{1... | collective-permute-start | bytes 1572872 | tf_op jit(solution)/shard_map/ppermute | solution.py:476
  87.9 12.3 %collective-permute-start.32 = (bf16[64,2048]{1,0:T(8,128)(2,1)S(1)}, bf16[64,2048]{1,0:T(8,128)(2,1)S(1)}, u32[]{:S(2)}, u32[]{:S(2)}) collective-permute-start(bf16[64,2048]{1,0:T(8,128)(2,1)S(1)} %add_convert_fusion.2), channel_id=1, source_target_pairs={{0,2},{1,3},{2,0},{3,1},{4,6},{5,7},{6,4},{7,5},{8,10},{9,11},{10,... | collective-permute-start | bytes 786440 | tf_op jit(solution)/shard_map/ppermute | solution.py:476
  95.2 21.4 %collective-permute-start.31 = (bf16[64,2048]{1,0:T(8,128)(2,1)S(1)}, bf16[64,2048]{1,0:T(8,128)(2,1)S(1)}, u32[]{:S(2)}, u32[]{:S(2)}) collective-permute-start(bf16[64,2048]{1,0:T(8,128)(2,1)S(1)} %add_convert_fusion.3), channel_id=1, source_target_pairs={{0,8},{4,12},{8,0},{12,4},{1,9},{5,13},{9,1},{13,5},{2,10},{6,14},... | collective-permute-start | bytes 786440 | tf_op jit(solution)/shard_map/ppermute | solution.py:476
  100.3 16.2 %collective-permute-start.33 = (bf16[64,2048]{1,0:T(8,128)(2,1)S(1)}, bf16[64,2048]{1,0:T(8,128)(2,1)S(1)}, u32[]{:S(2)}, u32[]{:S(2)}) collective-permute-start(bf16[64,2048]{1,0:T(8,128)(2,1)S(1)} %add_convert_fusion.1), channel_id=1, source_target_pairs={{0,12},{4,8},{8,4},{12,0},{1,13},{5,9},{9,5},{13,1},{2,14},{6,10},... | collective-permute-start | bytes 786440 | tf_op jit(solution)/shard_map/ppermute | solution.py:476
  105.4 11.1 %collective-permute-start.30 = (bf16[64,2048]{1,0:T(8,128)(2,1)S(1)}, bf16[64,2048]{1,0:T(8,128)(2,1)S(1)}, u32[]{:S(2)}, u32[]{:S(2)}) collective-permute-start(bf16[64,2048]{1,0:T(8,128)(2,1)S(1)} %slice.96), channel_id=1, source_target_pairs={{0,2},{1,3},{2,0},{3,1},{4,6},{5,7},{6,4},{7,5},{8,10},{9,11},{10,... | collective-permute-start | bytes 786440 | tf_op jit(solution)/shard_map/ppermute | solution.py:476
  (22 other events, 115.6 us)

commit v2 on v1

--- a/solution.py
+++ b/solution.py
@@ -387,30 +387,37 @@
     stat_ref[...] = stat
 
 
-def attend_last_kernel(kind, steps, *refs):
-    raw_refs, refs = refs[: len(steps)], refs[len(steps) :]
-    query_ref, small_ref, cos_ref, sin_ref, stat_ref, mixed_ref, proj_ref, *refs = refs
+def attend_last_kernel(kind, steps, row_sets, *refs):
+    count = len(steps) or 2
+    raw_refs, refs = refs[:count], refs[count:]
+    query_ref, small_ref, cos_ref, sin_ref, stat_ref, mixed_ref, *refs = refs
     lanes = small_ref.shape[1]
-    keys, values = kind[0](raw_refs, steps, small_ref, cos_ref, sin_ref)
+    if steps:
+        keys, values = kind[0](raw_refs, steps, small_ref, cos_ref, sin_ref)
+    else:
+        keys, values = [ref[...] for ref in raw_refs]
     scale = (lanes // kind[2]) ** -0.5
-    heads = []
-    for h, query in enumerate(kind[1](query_ref, lanes)):
-        before = (stat_ref[:, 2 * h : 2 * h + 1], stat_ref[:, 2 * h + 1 : 2 * h + 2], mixed_ref[h])
-        _, total, mixed = mixed_in(query, keys, values, scale, before)
-        heads.append(mixed / total)
-    if kind[2] == 1:
-        joined = jnp.concatenate(heads, axis=1)
-    else:
-        joined = jnp.where(lanes_of(heads[0].shape) < lanes // 2, heads[0], heads[1])
-    terms = jnp.dot(joined.astype(jnp.bfloat16), proj_ref[...], preferred_element_type=jnp.float32)
-    if len(refs) == 1:
-        refs[0][...] = terms
-        return
-    terms_ref, keep_ref, send_ref = refs
-    terms = (terms_ref[...] + terms).astype(jnp.bfloat16)
-    half = terms.shape[0] // 2
-    keep_ref[...] = terms[:half]
-    send_ref[...] = terms[half:]
+    queries = kind[1](query_ref, lanes)
+    outs = refs if kind[2] == 1 else refs[3:]
+    for rows, out_ref in zip(row_sets, outs):
+        heads = []
+        for h, query in enumerate(queries):
+            top, total = stat_ref[rows, 2 * h : 2 * h + 1], stat_ref[rows, 2 * h + 1 : 2 * h + 2]
+            before = (top, total, mixed_ref[h, rows])
+            _, total, mixed = mixed_in(query[rows], keys, values, scale, before)
+            heads.append(mixed / total)
+        if kind[2] == 1:
+            out_ref[...] = jnp.concatenate(heads, axis=1).astype(jnp.bfloat16)
+            continue
+        wide_ref, wide_proj_ref, narrow_proj_ref = refs[:3]
+        narrow = jnp.where(lanes_of(heads[0].shape) < lanes // 2, heads[0], heads[1])
+        terms = jnp.dot(wide_ref[rows, :], wide_proj_ref[...], preferred_element_type=jnp.float32)
+        terms = terms + jnp.dot(
+            narrow.astype(jnp.bfloat16), narrow_proj_ref[...], preferred_element_type=jnp.float32
+        )
+        out_ref[...] = terms.astype(jnp.bfloat16)
+    for value, ref in zip((keys, values), outs[len(row_sets) :]):
+        ref[...] = value
 
 
 def norm_kernel(res_ref, keep_ref, came_ref, crossed_ref, gain_ref, att_ref, normed_ref):
@@ -423,13 +430,13 @@
     normed_ref[...] = (state * rms(state, state.shape[1]) * gain_ref[...]).astype(jnp.bfloat16)
 
 
-def expert_kernel(r0_ref, r2_ref, r1_ref, r3_ref, gate_ref, up_ref, down_ref, keep_ref, send_ref):
-    rows = jnp.concatenate([ref[...] for ref in (r0_ref, r2_ref, r1_ref, r3_ref)], axis=0)
+def expert_kernel(ours_ref, theirs_ref, gate_ref, up_ref, down_ref, keep_ref, send_ref):
+    rows = jnp.concatenate([ours_ref[...], theirs_ref[...]], axis=0)
     gate_act = jnp.dot(rows, gate_ref[0], preferred_element_type=jnp.float32)
     up_act = jnp.dot(rows, up_ref[0], preferred_element_type=jnp.float32)
     hidden = (gate_act / (1.0 + jnp.exp(-gate_act)) * up_act).astype(jnp.bfloat16)
     piece = jnp.dot(hidden, down_ref[0], preferred_element_type=jnp.float32).astype(jnp.bfloat16)
-    half = piece.shape[0] // 2
+    half = ours_ref.shape[0]
     keep_ref[...] = piece[:half]
     send_ref[...] = piece[half:]
 
@@ -469,7 +476,6 @@
     lanes = query_gain_wide.shape[0]
     tokens = n_sp * tok_count
     order = [r for r in range(n_tp) if r % 2 == 0] + [r for r in range(n_tp) if r % 2]
-    half = tok_count // 2
 
     def across(value, axis, step):
         size = lax.axis_size(axis)
@@ -503,12 +509,12 @@
     )
     near, far = tuple(range(n_sp - 1)), (n_sp - 1,)
     parts = {
-        "wide": (WIDE, raw_wide, [q_wide, small] + tables[:2], output_wide),
-        "narrow": (NARROW, raw_narrow, [q_narrow, small] + tables[2:], output_narrow),
+        "wide": (WIDE, raw_wide, [q_wide, small] + tables[:2]),
+        "narrow": (NARROW, raw_narrow, [q_narrow, small] + tables[2:]),
     }
     cost = dict(flops=WAIT_FLOPS // 2, exps=4 * tok_count**2)
     states = {}
-    for name, (kind, raw, shared, _) in parts.items():
+    for name, (kind, raw, shared) in parts.items():
         heads = shared[0].shape[1] // lanes * kind[2]
         states[name] = on_core(
             functools.partial(attend_first_kernel, kind, near),
@@ -519,73 +525,84 @@
             raw[:-1] + shared,
             **cost,
         )
-    outs, terms = [like(tok_count, model_width, jnp.float32)], []
-    for name, (kind, raw, shared, proj) in parts.items():
-        terms = on_core(
-            functools.partial(attend_last_kernel, kind, far),
+
+    def last(name, row_sets, outs, extra, ready=None):
+        kind, raw, shared = parts[name]
+        steps, given = ((), ready) if ready else (far, raw[-1:])
+        return on_core(
+            functools.partial(attend_last_kernel, kind, steps, row_sets),
             outs,
-            [*raw[-1:], *shared, *states[name], proj, *terms],
+            [*given, *shared, *states[name], *extra],
             **cost,
         )
-        outs = [like(half, model_width)] * 2
-    keep, send = terms
+
+    ours, far_ours, others, far_others = [
+        slice(i * own_rows, (i + 1) * own_rows) for i in range(n_tp)
+    ]
+    wide = last("wide", [slice(None)], [like(*queries_wide.shape)], [])
+    extra, out = [*wide, output_wide, output_narrow], like(own_rows, model_width)
+    made = [like(tok_count, lanes)] * 2
+    send_far, *ready = last("narrow", [far_others], [out] + made, extra)
+    came_far = across(send_far, "tp", 1)
+    keep_far = last("narrow", [far_ours], [out], extra, ready)[0]
+    pair = keep_far.astype(jnp.float32) + came_far.astype(jnp.float32)
+    crossed = across(pair.astype(jnp.bfloat16), "tp", 2)
+    send, keep = last("narrow", [others, ours], [out] * 2, extra, ready)
     came = across(send, "tp", 1)
 
     experts = sp ^ jnp.arange(n_sp, dtype=route_ids.dtype)
     chosen = route_ids[:, :, None] == experts[None, None, :]
     own_weights = jnp.sum(jnp.where(chosen, route_weights[:, :, None], 0.0), axis=1)
-    own_weights = lax.optimization_barrier((own_weights, send))[0]
-    pair_weights = jnp.concatenate([own_weights, across(own_weights, "tp", 2)], axis=0)
-
-    def crossing(keep, came):
-        pair = keep[own_rows:].astype(jnp.float32) + came[own_rows:].astype(jnp.float32)
-        return across(pair.astype(jnp.bfloat16), "tp", 2)
+    own_weights = lax.optimization_barrier((own_weights, keep))[0]
+    beside_weights = across(own_weights, "tp", 2)
 
     attended, normed = on_core(
         norm_kernel,
         [like(own_rows, model_width)] * 2,
-        [residual, keep, came, crossing(keep, came), norm_gain[None, :]],
+        [residual, keep, came, crossed, norm_gain[None, :]],
         flops=WAIT_FLOPS,
     )
 
     arrived = spread(normed)
-    crossed_rows, keeps, cames = [], [], []
+
+    def expert_parts(rows):
+        other = across(rows, "tp", 1)
+        keep, send = on_core(
+            expert_kernel,
+            [like(own_rows, model_width)] * 2,
+            [rows, other, gate_weight, up_weight, down_weight],
+            flops=3 * tok_count * model_width * hidden_width,
+            exps=tok_count * hidden_width // 2,
+            vmem=12,
+        )
+        came = across(send, "tp", 1)
+        return keep.astype(jnp.float32) + came.astype(jnp.float32)
+
+    crossed_rows, ours, theirs = [], [], []
     for r in range(n_sp):
         if r % 2:
             crossed_rows.append(across(crossed_rows[r - 1], "sp", 1))
         else:
             crossed_rows.append(across(arrived[r], "tp", 2))
-        rows = [arrived[r], crossed_rows[r]]
-        rows = rows + [across(rows[0], "tp", 1), across(rows[1], "tp", 1)]
-        keep, send = on_core(
-            expert_kernel,
-            [like(half, model_width)] * 2,
-            rows + [gate_weight, up_weight, down_weight],
-            flops=6 * tok_count * model_width * hidden_width,
-            exps=tok_count * hidden_width,
-            vmem=12,
-        )
-        keeps.append(keep)
-        cames.append(across(send, "tp", 1))
-
-    def over_cores(r, rows=slice(None)):
-        return keeps[r][rows].astype(jnp.float32) + cames[r][rows].astype(jnp.float32)
-
-    beside = across(over_cores(1).astype(jnp.bfloat16), "sp", 1)
+        ours.append(expert_parts(arrived[r]))
+        theirs.append(expert_parts(crossed_rows[r]))
+
+    near = [across(v[1].astype(jnp.bfloat16), "sp", 1) for v in (ours, theirs)]
     gates, far_outs = [], []
     for r in range(2, n_sp):
-        theirs = over_cores(r, slice(own_rows, None)).astype(jnp.bfloat16)
-        crossed = across(theirs, "tp", 2).astype(jnp.float32)
-        expert_out = (over_cores(r, slice(own_rows)) + crossed).astype(jnp.bfloat16)
-        gates += [theirs] if far_outs else [theirs, expert_out]
-        far_outs.append(across(expert_out, "sp", r).astype(jnp.float32))
-
-    beside = lax.optimization_barrier((beside, *gates))[0].astype(jnp.float32)
-    near_sum = over_cores(0) * pair_weights[:, 0:1] + beside * pair_weights[:, 1:2]
-    crossed = across(near_sum[own_rows:].astype(jnp.bfloat16), "tp", 2)
-    total = attended.astype(jnp.float32) + near_sum[:own_rows] + crossed.astype(jnp.float32)
+        sent = theirs[r].astype(jnp.bfloat16)
+        crossed = across(sent, "tp", 2).astype(jnp.float32)
+        outcome = (ours[r] + crossed).astype(jnp.bfloat16)
+        gates += [sent] if r > 2 else [sent, outcome]
+        far_outs.append(across(outcome, "sp", r).astype(jnp.float32))
+
+    near = [v.astype(jnp.float32) for v in lax.optimization_barrier((*near, *gates))[:2]]
+    sent = theirs[0] * beside_weights[:, 0:1] + near[1] * beside_weights[:, 1:2]
+    crossed = across(sent.astype(jnp.bfloat16), "tp", 2).astype(jnp.float32)
+    total = attended.astype(jnp.float32) + crossed
+    total = total + ours[0] * own_weights[:, 0:1] + near[0] * own_weights[:, 1:2]
     for r, expert_out in enumerate(far_outs, 2):
-        total = total + pair_weights[:own_rows, r : r + 1] * expert_out
+        total = total + own_weights[:, r : r + 1] * expert_out
     return total.astype(jnp.bfloat16)
 
 

time: 119 us -> 129 us (1.084)
  starting transfers between devices: 25.7 us -> 34.9 us
  Pallas kernels: 22.8 us -> 26.3 us
  waiting for transfers between devices: 57.2 us -> 55.3 us
    ppermute x34 -> x40, starting transfers between devices: 25.7 us -> 34.9 us  [across(): return lax.ppermute(value, axis, [(i, i ^ step) for i in range(size)])]
    pallas_call x10 -> x16, Pallas kernels: 22.8 us -> 26.3 us  [on_core(): pl.pallas_call(kernel, out_shape=results, in_specs=[VMEM_SPEC] * len(args...]
    ppermute x34 -> x40, waiting for transfers between devices: 57.2 us -> 55.3 us  [across(): return lax.ppermute(value, axis, [(i, i ^ step) for i in range(size)])]
  transfers between devices with their start and end apart: 34 -> 40, of which waited for: 12 -> 13; matrix products, arithmetic and copies ran while one was open for 3% -> 3% of each run, Pallas kernels for 17% -> 19%
where the time goes in v2:
time: 129 us; the launch traced here: 128 us
  waiting for transfers between devices  55.3 us (43%)
  starting transfers between devices  34.9 us (27%)
  Pallas kernels  26.3 us (20%)
  local copies, waits for them, and re-layouts  7.18 us (6%)
  other arithmetic  4.43 us (3%)
    ppermute x40, waiting for transfers between devices, across(): return lax.ppermute(value, axis, [(i, i ^ step) for i in range(size)])  55.3 us
    ppermute x40, starting transfers between devices, across(): return lax.ppermute(value, axis, [(i, i ^ step) for i in range(size)])  34.9 us
    pallas_call x16, Pallas kernels, on_core(): pl.pallas_call(kernel, out_shape=results, in_specs=[VMEM_SPEC] * len(args...  26.3 us
    unnamed x24, local copies, waits for them, and re-layouts  6.32 us
  transfers between devices with their start and end apart: 40, of which 13 were waited for; matrix products, arithmetic and copies ran while one was open for 3% of the time, Pallas kernels for 19%

profile of v2, /device:TPU:0, one launch (start us, length us, event | category | flops | bytes accessed | tf_op | source)
XLA Modules:
  0.0 128.5 jit_solution(7800845513430338707)
XLA Ops:
  0.9 4.1 %collective-permute-start.3 = (bf16[512,128]{1,0:T(8,128)(2,1)S(1)}, bf16[512,128]{1,0:T(8,128)(2,1)S(1)}, u32[]{:S(2)}, u32[]{:S(2)}) collective-permute-start(bf16[512,128]{1,0:T(8,128)(2,1)S(1)} %pad_maximum_fusion.1.refs_0_), channel_id=1, source_target_pairs={{0,8},{4,12},{8,0},{12,4},{1,9},{5,13},{9,1},{13,5},{2,10},{6,14},... | collective-permute-start | bytes 393224 | tf_op jit(solution)/shard_map/ppermute | solution.py:482
  11.2 2.3 %collective-permute-done.refs_2_ = bf16[128,256]{1,0:T(8,128)(2,1)S(1)} collective-permute-done((bf16[128,256]{1,0:T(8,128)(2,1)S(1)}, bf16[128,256]{1,0:T(8,128)(2,1)S(1)}, u32[]{:S(2)}, u32[]{:S(2)}) %collective-permute-start) | collective-permute-done | bytes 65568 | tf_op jit(solution)/shard_map/ppermute | solution.py:482
  19.3 2.7 %collective-permute-done.4.refs_0_ = bf16[512,128]{1,0:T(8,128)(2,1)S(1)} collective-permute-done((bf16[512,128]{1,0:T(8,128)(2,1)S(1)}, bf16[512,128]{1,0:T(8,128)(2,1)S(1)}, u32[]{:S(2)}, u32[]{:S(2)}) %collective-permute-start.4) | collective-permute-done | bytes 131104 | tf_op jit(solution)/shard_map/ppermute | solution.py:482
  25.0 2.2 %shard_map.204 = (bf16[64,2048]{1,0:T(8,128)(2,1)S(1)}, bf16[64,2048]{1,0:T(8,128)(2,1)S(1)}) custom-call(bf16[256,128]{1,0:T(8,128)(2,1)S(1)} %get-tuple-element.51.refs_0_, bf16[256,128]{1,0:T(8,128)(2,1)S(1)} %get-tuple-element.52.refs_1_, bf16[256,128]{1,0:T(8,128)(2,1)S(1)} %get-tuple-element.41.refs_3_.refs_1_.refs_2_, f32[6,128]{1,0:T(8,128)S(1)} %bitcast.21, ...), custom_call_target="tpu_custom_call" | custom-call | flops 4000000000 | bytes 3869696 | tf_op jit(solution)/shard_map/pallas_call | solution.py:225
  30.6 6.7 %collective-permute-done.8.crossed_ref = bf16[64,2048]{1,0:T(8,128)(2,1)S(1)} collective-permute-done((bf16[64,2048]{1,0:T(8,128)(2,1)S(1)}, bf16[64,2048]{1,0:T(8,128)(2,1)S(1)}, u32[]{:S(2)}, u32[]{:S(2)}) %collective-permute-start.8) | collective-permute-done | bytes 262176 | tf_op jit(solution)/shard_map/ppermute | solution.py:482
  38.5 2.8 %collective-permute-start.21 = (bf16[64,2048]{1,0:T(8,128)(2,1)S(1)}, bf16[64,2048]{1,0:T(8,128)(2,1)S(1)}, u32[]{:S(2)}, u32[]{:S(2)}) collective-permute-start(bf16[64,2048]{1,0:T(8,128)(2,1)S(1)} %get-tuple-element.57.ours_ref), channel_id=1, source_target_pairs={{0,8},{4,12},{8,0},{12,4},{1,9},{5,13},{9,1},{13,5},{2,10},{6,14},... | collective-permute-start | bytes 786440 | tf_op jit(solution)/shard_map/ppermute | solution.py:482
  43.5 7.3 %collective-permute-done.13.ours_ref = bf16[64,2048]{1,0:T(8,128)(2,1)S(1)} collective-permute-done((bf16[64,2048]{1,0:T(8,128)(2,1)S(1)}, bf16[64,2048]{1,0:T(8,128)(2,1)S(1)}, u32[]{:S(2)}, u32[]{:S(2)}) %collective-permute-start.13) | collective-permute-done | bytes 262176 | tf_op jit(solution)/shard_map/ppermute | solution.py:482
  51.3 2.0 %copy-done = bf16[1,2048,896]{2,1,0:T(8,128)(2,1)S(1)} copy-done((bf16[1,2048,896]{2,1,0:T(8,128)(2,1)S(1)}, bf16[1,2048,896]{2,1,0:T(8,128)(2,1)}, u32[]{:S(2)}) %copy-start) | copy-done | bytes 3670040
  53.4 2.0 %copy-done.2 = bf16[1,2048,896]{2,1,0:T(8,128)(2,1)S(1)} copy-done((bf16[1,2048,896]{2,1,0:T(8,128)(2,1)S(1)}, bf16[1,2048,896]{2,1,0:T(8,128)(2,1)}, u32[]{:S(2)}) %copy-start.2) | copy-done | bytes 3670040
  55.4 2.0 %copy-done.4 = bf16[1,896,2048]{2,1,0:T(8,128)(2,1)S(1)} copy-done((bf16[1,896,2048]{2,1,0:T(8,128)(2,1)S(1)}, bf16[1,896,2048]{2,1,0:T(8,128)(2,1)}, u32[]{:S(2)}) %copy-start.4) | copy-done | bytes 3670040
  57.4 1.9 %shard_map.213 = (bf16[64,2048]{1,0:T(8,128)(2,1)S(1)}, bf16[64,2048]{1,0:T(8,128)(2,1)S(1)}) custom-call(bf16[64,2048]{1,0:T(8,128)(2,1)S(1)} %get-tuple-element.57.ours_ref, bf16[64,2048]{1,0:T(8,128)(2,1)S(1)} %collective-permute-done.32.theirs_ref, bf16[1,2048,896]{2,1,0:T(8,128)(2,1)S(1)} %copy-done, bf16[1,2048,896]{2,1,0:T(8,128)(2,1)S(1)} %copy-done.2, ...), custom_call_target="tpu_custom_call" | custom-call | flops 1409286144 | bytes 12058624 | tf_op jit(solution)/shard_map/pallas_call | solution.py:225
  61.0 3.1 %collective-permute-start.17 = (bf16[64,2048]{1,0:T(8,128)(2,1)S(1)}, bf16[64,2048]{1,0:T(8,128)(2,1)S(1)}, u32[]{:S(2)}, u32[]{:S(2)}) collective-permute-start(bf16[64,2048]{1,0:T(8,128)(2,1)S(1)} %collective-permute-done.9.ours_ref), channel_id=1, source_target_pairs={{0,4},{4,0},{8,12},{12,8},{1,5},{5,1},{9,13},{13,9},{2,6},{6,2},{1... | collective-permute-start | bytes 786440 | tf_op jit(solution)/shard_map/ppermute | solution.py:482
  64.1 2.0 %shard_map.208 = (bf16[64,2048]{1,0:T(8,128)(2,1)S(1)}, bf16[64,2048]{1,0:T(8,128)(2,1)S(1)}) custom-call(bf16[64,2048]{1,0:T(8,128)(2,1)S(1)} %collective-permute-done.13.ours_ref, bf16[64,2048]{1,0:T(8,128)(2,1)S(1)} %collective-permute-done.14.theirs_ref, bf16[1,2048,896]{2,1,0:T(8,128)(2,1)S(1)} %copy-done.1, bf16[1,2048,896]{2,1,0:T(8,128)(2,1)S(1)} %copy-done.3, ...), custom_call_target="tpu_custom_call" | custom-call | flops 1409286144 | bytes 12058624 | tf_op jit(solution)/shard_map/pallas_call | solution.py:225
  66.7 1.9 %shard_map.211 = (bf16[64,2048]{1,0:T(8,128)(2,1)S(1)}, bf16[64,2048]{1,0:T(8,128)(2,1)S(1)}) custom-call(bf16[64,2048]{1,0:T(8,128)(2,1)S(1)} %collective-permute-done.21.ours_ref, bf16[64,2048]{1,0:T(8,128)(2,1)S(1)} %collective-permute-done.25.theirs_ref, bf16[1,2048,896]{2,1,0:T(8,128)(2,1)S(1)} %copy-done.1, bf16[1,2048,896]{2,1,0:T(8,128)(2,1)S(1)} %copy-done.3, ...), custom_call_target="tpu_custom_call" | custom-call | flops 1409286144 | bytes 12058624 | tf_op jit(solution)/shard_map/pallas_call | solution.py:225
  68.9 1.9 %shard_map.207 = (bf16[64,2048]{1,0:T(8,128)(2,1)S(1)}, bf16[64,2048]{1,0:T(8,128)(2,1)S(1)}) custom-call(bf16[64,2048]{1,0:T(8,128)(2,1)S(1)} %collective-permute-done.9.ours_ref, bf16[64,2048]{1,0:T(8,128)(2,1)S(1)} %collective-permute-done.10.theirs_ref, bf16[1,2048,896]{2,1,0:T(8,128)(2,1)S(1)} %copy-done.1, bf16[1,2048,896]{2,1,0:T(8,128)(2,1)S(1)} %copy-done.3, ...), custom_call_target="tpu_custom_call" | custom-call | flops 1409286144 | bytes 12058624 | tf_op jit(solution)/shard_map/pallas_call | solution.py:225
  71.6 5.4 %collective-permute-done.35.ours_ref = bf16[64,2048]{1,0:T(8,128)(2,1)S(1)} collective-permute-done((bf16[64,2048]{1,0:T(8,128)(2,1)S(1)}, bf16[64,2048]{1,0:T(8,128)(2,1)S(1)}, u32[]{:S(2)}, u32[]{:S(2)}) %collective-permute-start.35) | collective-permute-done | bytes 262176 | tf_op jit(solution)/shard_map/ppermute | solution.py:482
  80.2 1.9 %shard_map.209 = (bf16[64,2048]{1,0:T(8,128)(2,1)S(1)}, bf16[64,2048]{1,0:T(8,128)(2,1)S(1)}) custom-call(bf16[64,2048]{1,0:T(8,128)(2,1)S(1)} %collective-permute-done.17.ours_ref, bf16[64,2048]{1,0:T(8,128)(2,1)S(1)} %collective-permute-done.18.theirs_ref, bf16[1,2048,896]{2,1,0:T(8,128)(2,1)S(1)} %copy-done.1, bf16[1,2048,896]{2,1,0:T(8,128)(2,1)S(1)} %copy-done.3, ...), custom_call_target="tpu_custom_call" | custom-call | flops 1409286144 | bytes 12058624 | tf_op jit(solution)/shard_map/pallas_call | solution.py:225
  87.7 1.9 %shard_map.212 = (bf16[64,2048]{1,0:T(8,128)(2,1)S(1)}, bf16[64,2048]{1,0:T(8,128)(2,1)S(1)}) custom-call(bf16[64,2048]{1,0:T(8,128)(2,1)S(1)} %collective-permute-done.28.ours_ref, bf16[64,2048]{1,0:T(8,128)(2,1)S(1)} %collective-permute-done.29.theirs_ref, bf16[1,2048,896]{2,1,0:T(8,128)(2,1)S(1)} %copy-done.1, bf16[1,2048,896]{2,1,0:T(8,128)(2,1)S(1)} %copy-done.3, ...), custom_call_target="tpu_custom_call" | custom-call | flops 1409286144 | bytes 12058624 | tf_op jit(solution)/shard_map/pallas_call | solution.py:225
  89.7 4.7 %collective-permute-done.27 = bf16[64,2048]{1,0:T(8,128)(2,1)S(1)} collective-permute-done((bf16[64,2048]{1,0:T(8,128)(2,1)S(1)}, bf16[64,2048]{1,0:T(8,128)(2,1)S(1)}, u32[]{:S(2)}, u32[]{:S(2)}) %collective-permute-start.27) | collective-permute-done | bytes 262176 | tf_op jit(solution)/shard_map/ppermute | solution.py:482
  97.2 2.8 %collective-permute-start.34 = (bf16[64,2048]{1,0:T(8,128)(2,1)S(1)}, bf16[64,2048]{1,0:T(8,128)(2,1)S(1)}, u32[]{:S(2)}, u32[]{:S(2)}) collective-permute-start(bf16[64,2048]{1,0:T(8,128)(2,1)S(1)} %add_convert_fusion.4), channel_id=1, source_target_pairs={{0,8},{4,12},{8,0},{12,4},{1,9},{5,13},{9,1},{13,5},{2,10},{6,14},... | collective-permute-start | bytes 786440 | tf_op jit(solution)/shard_map/ppermute | solution.py:482
  99.9 9.9 %collective-permute-done.20 = bf16[64,2048]{1,0:T(8,128)(2,1)S(1)} collective-permute-done((bf16[64,2048]{1,0:T(8,128)(2,1)S(1)}, bf16[64,2048]{1,0:T(8,128)(2,1)S(1)}, u32[]{:S(2)}, u32[]{:S(2)}) %collective-permute-start.20) | collective-permute-done | bytes 262176 | tf_op jit(solution)/shard_map/ppermute | solution.py:482
  112.1 6.9 %collective-permute-done.38 = bf16[64,2048]{1,0:T(8,128)(2,1)S(1)} collective-permute-done((bf16[64,2048]{1,0:T(8,128)(2,1)S(1)}, bf16[64,2048]{1,0:T(8,128)(2,1)S(1)}, u32[]{:S(2)}, u32[]{:S(2)}) %collective-permute-start.38) | collective-permute-done | bytes 262176 | tf_op jit(solution)/shard_map/ppermute | solution.py:482
  120.7 2.2 %collective-permute-done.31 = bf16[64,2048]{1,0:T(8,128)(2,1)S(1)} collective-permute-done((bf16[64,2048]{1,0:T(8,128)(2,1)S(1)}, bf16[64,2048]{1,0:T(8,128)(2,1)S(1)}, u32[]{:S(2)}, u32[]{:S(2)}) %collective-permute-start.31) | collective-permute-done | bytes 262176 | tf_op jit(solution)/shard_map/ppermute | solution.py:482
  122.9 4.5 %collective-permute-done.39 = bf16[64,2048]{1,0:T(8,128)(2,1)S(1)} collective-permute-done((bf16[64,2048]{1,0:T(8,128)(2,1)S(1)}, bf16[64,2048]{1,0:T(8,128)(2,1)S(1)}, u32[]{:S(2)}, u32[]{:S(2)}) %collective-permute-start.39) | collective-permute-done | bytes 262176 | tf_op jit(solution)/shard_map/ppermute | solution.py:482
  (113 shorter events, 43.1 us)
Async XLA Ops:
  0.9 16.1 %collective-permute-start.3 = (bf16[512,128]{1,0:T(8,128)(2,1)S(1)}, bf16[512,128]{1,0:T(8,128)(2,1)S(1)}, u32[]{:S(2)}, u32[]{:S(2)}) collective-permute-start(bf16[512,128]{1,0:T(8,128)(2,1)S(1)} %pad_maximum_fusion.1.refs_0_), channel_id=1, source_target_pairs={{0,8},{4,12},{8,0},{12,4},{1,9},{5,13},{9,1},{13,5},{2,10},{6,14},... | collective-permute-start | bytes 393224 | tf_op jit(solution)/shard_map/ppermute | solution.py:482
  5.0 12.8 %collective-permute-start.5 = (bf16[512,128]{1,0:T(8,128)(2,1)S(1)}, bf16[512,128]{1,0:T(8,128)(2,1)S(1)}, u32[]{:S(2)}, u32[]{:S(2)}) collective-permute-start(bf16[512,128]{1,0:T(8,128)(2,1)S(1)} %pad_maximum_fusion.1.refs_0_), channel_id=1, source_target_pairs={{0,4},{4,0},{8,12},{12,8},{1,5},{5,1},{9,13},{13,9},{2,6},{6,2},{1... | collective-permute-start | bytes 393224 | tf_op jit(solution)/shard_map/ppermute | solution.py:482
  13.4 9.7 %collective-permute-start.1 = (bf16[128,256]{1,0:T(8,128)(2,1)S(1)}, bf16[128,256]{1,0:T(8,128)(2,1)S(1)}, u32[]{:S(2)}, u32[]{:S(2)}) collective-permute-start(bf16[128,256]{1,0:T(8,128)(2,1)S(1)} %collective-permute-done.refs_2_), channel_id=1, source_target_pairs={{0,4},{4,0},{8,12},{12,8},{1,5},{5,1},{9,13},{13,9},{2,6},{6,2},{1... | collective-permute-start | bytes 196616 | tf_op jit(solution)/shard_map/ppermute | solution.py:482
  37.7 13.1 %collective-permute-start.13 = (bf16[64,2048]{1,0:T(8,128)(2,1)S(1)}, bf16[64,2048]{1,0:T(8,128)(2,1)S(1)}, u32[]{:S(2)}, u32[]{:S(2)}) collective-permute-start(bf16[64,2048]{1,0:T(8,128)(2,1)S(1)} %get-tuple-element.57.ours_ref), channel_id=1, source_target_pairs={{0,4},{4,0},{8,12},{12,8},{1,5},{5,1},{9,13},{13,9},{2,6},{6,2},{1... | collective-permute-start | bytes 786440 | tf_op jit(solution)/shard_map/ppermute | solution.py:482
  38.5 12.2 %collective-permute-start.21 = (bf16[64,2048]{1,0:T(8,128)(2,1)S(1)}, bf16[64,2048]{1,0:T(8,128)(2,1)S(1)}, u32[]{:S(2)}, u32[]{:S(2)}) collective-permute-start(bf16[64,2048]{1,0:T(8,128)(2,1)S(1)} %get-tuple-element.57.ours_ref), channel_id=1, source_target_pairs={{0,8},{4,12},{8,0},{12,4},{1,9},{5,13},{9,1},{13,5},{2,10},{6,14},... | collective-permute-start | bytes 786440 | tf_op jit(solution)/shard_map/ppermute | solution.py:482
  41.3 10.0 %collective-permute-start.32 = (bf16[64,2048]{1,0:T(8,128)(2,1)S(1)}, bf16[64,2048]{1,0:T(8,128)(2,1)S(1)}, u32[]{:S(2)}, u32[]{:S(2)}) collective-permute-start(bf16[64,2048]{1,0:T(8,128)(2,1)S(1)} %get-tuple-element.57.ours_ref), channel_id=1, source_target_pairs={{0,1},{1,0},{2,3},{3,2},{4,5},{5,4},{6,7},{7,6},{8,9},{9,8},{10,11... | collective-permute-start | bytes 786440 | tf_op jit(solution)/shard_map/ppermute | solution.py:482
  41.4 9.3 %collective-permute-start.12 = (f32[64,4]{0,1:T(4,128)S(1)}, f32[64,4]{0,1:T(4,128)S(1)}, u32[]{:S(2)}, u32[]{:S(2)}) collective-permute-start(f32[64,4]{0,1:T(4,128)S(1)} %select_reduce_fusion), channel_id=1, source_target_pairs={{0,2},{1,3},{2,0},{3,1},{4,6},{5,7},{6,4},{7,5},{8,10},{9,11},{10,... | collective-permute-start | bytes 3080 | tf_op jit(solution)/shard_map/ppermute | solution.py:482
  42.9 18.0 %collective-permute-start.9 = (bf16[64,2048]{1,0:T(8,128)(2,1)S(1)}, bf16[64,2048]{1,0:T(8,128)(2,1)S(1)}, u32[]{:S(2)}, u32[]{:S(2)}) collective-permute-start(bf16[64,2048]{1,0:T(8,128)(2,1)S(1)} %get-tuple-element.57.ours_ref), channel_id=1, source_target_pairs={{0,2},{1,3},{2,0},{3,1},{4,6},{5,7},{6,4},{7,5},{8,10},{9,11},{10,... | collective-permute-start | bytes 786440 | tf_op jit(solution)/shard_map/ppermute | solution.py:482
  50.7 13.4 %collective-permute-start.14 = (bf16[64,2048]{1,0:T(8,128)(2,1)S(1)}, bf16[64,2048]{1,0:T(8,128)(2,1)S(1)}, u32[]{:S(2)}, u32[]{:S(2)}) collective-permute-start(bf16[64,2048]{1,0:T(8,128)(2,1)S(1)} %collective-permute-done.13.ours_ref), channel_id=1, source_target_pairs={{0,1},{1,0},{2,3},{3,2},{4,5},{5,4},{6,7},{7,6},{8,9},{9,8},{10,11... | collective-permute-start | bytes 786440 | tf_op jit(solution)/shard_map/ppermute | solution.py:482
  50.7 15.4 %collective-permute-start.25 = (bf16[64,2048]{1,0:T(8,128)(2,1)S(1)}, bf16[64,2048]{1,0:T(8,128)(2,1)S(1)}, u32[]{:S(2)}, u32[]{:S(2)}) collective-permute-start(bf16[64,2048]{1,0:T(8,128)(2,1)S(1)} %collective-permute-done.21.ours_ref), channel_id=1, source_target_pairs={{0,1},{1,0},{2,3},{3,2},{4,5},{5,4},{6,7},{7,6},{8,9},{9,8},{10,11... | collective-permute-start | bytes 786440 | tf_op jit(solution)/shard_map/ppermute | solution.py:482
  59.3 61.4 %collective-permute-start.33 = (bf16[64,2048]{1,0:T(8,128)(2,1)S(1)}, bf16[64,2048]{1,0:T(8,128)(2,1)S(1)}, u32[]{:S(2)}, u32[]{:S(2)}) collective-permute-start(bf16[64,2048]{1,0:T(8,128)(2,1)S(1)} %get-tuple-element.73), channel_id=1, source_target_pairs={{0,1},{1,0},{2,3},{3,2},{4,5},{5,4},{6,7},{7,6},{8,9},{9,8},{10,11... | collective-permute-start | bytes 786440 | tf_op jit(solution)/shard_map/ppermute | solution.py:482
  59.4 11.5 %collective-permute-start.22 = (bf16[64,2048]{1,0:T(8,128)(2,1)S(1)}, bf16[64,2048]{1,0:T(8,128)(2,1)S(1)}, u32[]{:S(2)}, u32[]{:S(2)}) collective-permute-start(bf16[64,2048]{1,0:T(8,128)(2,1)S(1)} %collective-permute-done.21.ours_ref), channel_id=1, source_target_pairs={{0,2},{1,3},{2,0},{3,1},{4,6},{5,7},{6,4},{7,5},{8,10},{9,11},{10,... | collective-permute-start | bytes 786440 | tf_op jit(solution)/shard_map/ppermute | solution.py:482
  61.0 9.9 %collective-permute-start.17 = (bf16[64,2048]{1,0:T(8,128)(2,1)S(1)}, bf16[64,2048]{1,0:T(8,128)(2,1)S(1)}, u32[]{:S(2)}, u32[]{:S(2)}) collective-permute-start(bf16[64,2048]{1,0:T(8,128)(2,1)S(1)} %collective-permute-done.9.ours_ref), channel_id=1, source_target_pairs={{0,4},{4,0},{8,12},{12,8},{1,5},{5,1},{9,13},{13,9},{2,6},{6,2},{1... | collective-permute-start | bytes 786440 | tf_op jit(solution)/shard_map/ppermute | solution.py:482
  70.8 18.8 %collective-permute-start.26 = (bf16[64,2048]{1,0:T(8,128)(2,1)S(1)}, bf16[64,2048]{1,0:T(8,128)(2,1)S(1)}, u32[]{:S(2)}, u32[]{:S(2)}) collective-permute-start(bf16[64,2048]{1,0:T(8,128)(2,1)S(1)} %get-tuple-element.68), channel_id=1, source_target_pairs={{0,1},{1,0},{2,3},{3,2},{4,5},{5,4},{6,7},{7,6},{8,9},{9,8},{10,11... | collective-permute-start | bytes 786440 | tf_op jit(solution)/shard_map/ppermute | solution.py:482
  70.9 8.7 %collective-permute-start.18 = (bf16[64,2048]{1,0:T(8,128)(2,1)S(1)}, bf16[64,2048]{1,0:T(8,128)(2,1)S(1)}, u32[]{:S(2)}, u32[]{:S(2)}) collective-permute-start(bf16[64,2048]{1,0:T(8,128)(2,1)S(1)} %collective-permute-done.17.ours_ref), channel_id=1, source_target_pairs={{0,1},{1,0},{2,3},{3,2},{4,5},{5,4},{6,7},{7,6},{8,9},{9,8},{10,11... | collective-permute-start | bytes 786440 | tf_op jit(solution)/shard_map/ppermute | solution.py:482
  82.1 28.7 %collective-permute-start.11 = (bf16[64,2048]{1,0:T(8,128)(2,1)S(1)}, bf16[64,2048]{1,0:T(8,128)(2,1)S(1)}, u32[]{:S(2)}, u32[]{:S(2)}) collective-permute-start(bf16[64,2048]{1,0:T(8,128)(2,1)S(1)} %get-tuple-element.59), channel_id=1, source_target_pairs={{0,1},{1,0},{2,3},{3,2},{4,5},{5,4},{6,7},{7,6},{8,9},{9,8},{10,11... | collective-permute-start | bytes 786440 | tf_op jit(solution)/shard_map/ppermute | solution.py:482
  85.8 8.5 %collective-permute-start.27 = (bf16[64,2048]{1,0:T(8,128)(2,1)S(1)}, bf16[64,2048]{1,0:T(8,128)(2,1)S(1)}, u32[]{:S(2)}, u32[]{:S(2)}) collective-permute-start(bf16[64,2048]{1,0:T(8,128)(2,1)S(1)} %add_convert_fusion.5), channel_id=1, source_target_pairs={{0,2},{1,3},{2,0},{3,1},{4,6},{5,7},{6,4},{7,5},{8,10},{9,11},{10,... | collective-permute-start | bytes 786440 | tf_op jit(solution)/shard_map/ppermute | solution.py:482
  86.7 10.4 %collective-permute-start.16 = (bf16[64,2048]{1,0:T(8,128)(2,1)S(1)}, bf16[64,2048]{1,0:T(8,128)(2,1)S(1)}, u32[]{:S(2)}, u32[]{:S(2)}) collective-permute-start(bf16[64,2048]{1,0:T(8,128)(2,1)S(1)} %add_convert_fusion.7), channel_id=1, source_target_pairs={{0,4},{4,0},{8,12},{12,8},{1,5},{5,1},{9,13},{13,9},{2,6},{6,2},{1... | collective-permute-start | bytes 786440 | tf_op jit(solution)/shard_map/ppermute | solution.py:482
  89.6 22.5 %collective-permute-start.37 = (bf16[64,2048]{1,0:T(8,128)(2,1)S(1)}, bf16[64,2048]{1,0:T(8,128)(2,1)S(1)}, u32[]{:S(2)}, u32[]{:S(2)}) collective-permute-start(bf16[64,2048]{1,0:T(8,128)(2,1)S(1)} %get-tuple-element.76), channel_id=1, source_target_pairs={{0,1},{1,0},{2,3},{3,2},{4,5},{5,4},{6,7},{7,6},{8,9},{9,8},{10,11... | collective-permute-start | bytes 786440 | tf_op jit(solution)/shard_map/ppermute | solution.py:482
  95.9 14.0 %collective-permute-start.20 = (bf16[64,2048]{1,0:T(8,128)(2,1)S(1)}, bf16[64,2048]{1,0:T(8,128)(2,1)S(1)}, u32[]{:S(2)}, u32[]{:S(2)}) collective-permute-start(bf16[64,2048]{1,0:T(8,128)(2,1)S(1)} %add_convert_fusion.6), channel_id=1, source_target_pairs={{0,4},{4,0},{8,12},{12,8},{1,5},{5,1},{9,13},{13,9},{2,6},{6,2},{1... | collective-permute-start | bytes 786440 | tf_op jit(solution)/shard_map/ppermute | solution.py:482
  97.2 25.8 %collective-permute-start.34 = (bf16[64,2048]{1,0:T(8,128)(2,1)S(1)}, bf16[64,2048]{1,0:T(8,128)(2,1)S(1)}, u32[]{:S(2)}, u32[]{:S(2)}) collective-permute-start(bf16[64,2048]{1,0:T(8,128)(2,1)S(1)} %add_convert_fusion.4), channel_id=1, source_target_pairs={{0,8},{4,12},{8,0},{12,4},{1,9},{5,13},{9,1},{13,5},{2,10},{6,14},... | collective-permute-start | bytes 786440 | tf_op jit(solution)/shard_map/ppermute | solution.py:482
  109.8 9.2 %collective-permute-start.38 = (bf16[64,2048]{1,0:T(8,128)(2,1)S(1)}, bf16[64,2048]{1,0:T(8,128)(2,1)S(1)}, u32[]{:S(2)}, u32[]{:S(2)}) collective-permute-start(bf16[64,2048]{1,0:T(8,128)(2,1)S(1)} %add_convert_fusion.3), channel_id=1, source_target_pairs={{0,2},{1,3},{2,0},{3,1},{4,6},{5,7},{6,4},{7,5},{8,10},{9,11},{10,... | collective-permute-start | bytes 786440 | tf_op jit(solution)/shard_map/ppermute | solution.py:482
  110.9 12.0 %collective-permute-start.31 = (bf16[64,2048]{1,0:T(8,128)(2,1)S(1)}, bf16[64,2048]{1,0:T(8,128)(2,1)S(1)}, u32[]{:S(2)}, u32[]{:S(2)}) collective-permute-start(bf16[64,2048]{1,0:T(8,128)(2,1)S(1)} %add_convert_fusion.2), channel_id=1, source_target_pairs={{0,2},{1,3},{2,0},{3,1},{4,6},{5,7},{6,4},{7,5},{8,10},{9,11},{10,... | collective-permute-start | bytes 786440 | tf_op jit(solution)/shard_map/ppermute | solution.py:482
  119.1 8.3 %collective-permute-start.39 = (bf16[64,2048]{1,0:T(8,128)(2,1)S(1)}, bf16[64,2048]{1,0:T(8,128)(2,1)S(1)}, u32[]{:S(2)}, u32[]{:S(2)}) collective-permute-start(bf16[64,2048]{1,0:T(8,128)(2,1)S(1)} %add_convert_fusion.1), channel_id=1, source_target_pairs={{0,12},{4,8},{8,4},{12,0},{1,13},{5,9},{9,5},{13,1},{2,14},{6,10},... | collective-permute-start | bytes 786440 | tf_op jit(solution)/shard_map/ppermute | solution.py:482
  (28 other events, 137.4 us)
